TPU v7x, 32 devices: a whole 2x2x4 slice. The times are simulated.
32 devices in a mesh: sp: 8 (over z, x), tp: 4 (over y, core).
Axes of the slice: x: 2, y: 2, z: 4, core: 2. Of those that a mesh axis runs over, the one named last changes fastest.
Arguments:
- tokens: bfloat16 [8192, 4096], P(('sp', 'tp')), may hold values from -6 to 6
- norm_gain: float32 [4096], replicated, may hold values from 0.1 to 1.9
- q_down: bfloat16 [4096, 768], replicated, may hold values from -0.09375 to 0.09375
- kv_down: bfloat16 [4096, 512], replicated, may hold values from -0.09375 to 0.09375
- rope_down: bfloat16 [4096, 32], replicated, may hold values from -8 to 8
- q_gain: float32 [768], replicated, may hold values from 0.1 to 1.9
- kv_gain: float32 [512], replicated, may hold values from 0.1 to 1.9
- q_up: bfloat16 [768, 1536], P(None, 'tp'), may hold values from -0.21875 to 0.21875
- kv_up: bfloat16 [512, 2048], P(None, 'tp'), may hold values from -0.25 to 0.25
- out_weight: bfloat16 [1024, 4096], replicated, may hold values from -0.1875 to 0.1875
- out_gain: float32 [4096], replicated, may hold values from 0.1 to 1.9
Outputs:
- mixed: bfloat16 [8192, 4096], P(('sp', 'tp'))
All inputs are finite; a program needn't handle non-finite values.
Results may differ from a plain program's by a relative error of at most 0.02.
The roundings to bfloat16 on the way count: a program that leaves them out, or rounds other values in their place, can miss the bound.
Values may be sent and summed in bfloat16 or wider, within the bound.
A program may use at most 128 MiB of HBM per device.

v0:
```python
import jax
import jax.numpy as jnp
from jax import lax
from jax.sharding import PartitionSpec as P

NOPE = 64
ROPE = 32
VDIM = 64


EPS = 1e-06
THETA = 500000.0


def scaled_norm(values_in, gain):
    values_in = values_in.astype(jnp.float32)
    return (
        values_in * lax.rsqrt(jnp.mean(values_in * values_in, axis=-1, keepdims=True) + EPS) * gain
    )


def rotate(values_in, position):
    width = values_in.shape[-1]
    half_dim = width // 2
    inverse = 1.0 / THETA ** (jnp.arange(0, width, 2, dtype=jnp.float32) / width)
    angles = position[:, None] * inverse[None, :]
    angles = angles.reshape((angles.shape[0],) + (1,) * (values_in.ndim - 2) + (half_dim,))
    cosine = jnp.cos(angles)
    sine = jnp.sin(angles)
    left = values_in[..., :half_dim]
    right = values_in[..., half_dim:]
    return jnp.concatenate([left * cosine - right * sine, right * cosine + left * sine], axis=-1)


def local(
    tokens,
    norm_gain,
    q_down,
    kv_down,
    rope_down,
    q_gain,
    kv_gain,
    q_up,
    kv_up,
    out_weight,
    out_gain,
):
    row_count = tokens.shape[0]
    tp_count = lax.axis_size("tp")
    tp_place = lax.axis_index("tp")
    sp_place = lax.axis_index("sp")
    group_rows = row_count * tp_count
    row_first = (sp_place * tp_count + tp_place) * row_count
    own_position = (row_first + jnp.arange(row_count)).astype(jnp.float32)
    normed = scaled_norm(tokens, norm_gain).astype(jnp.bfloat16)
    q_lat = scaled_norm(jnp.dot(normed, q_down, preferred_element_type=jnp.float32), q_gain).astype(
        jnp.bfloat16
    )
    kv_lat = scaled_norm(
        jnp.dot(normed, kv_down, preferred_element_type=jnp.float32), kv_gain
    ).astype(jnp.bfloat16)
    key_rot = rotate(
        jnp.dot(normed, rope_down, preferred_element_type=jnp.float32), own_position
    ).astype(jnp.bfloat16)
    q_group, kv_group, rot_group = (
        lax.all_gather(q_lat, "tp", axis=0, tiled=True),
        lax.all_gather(kv_lat, "tp", axis=0, tiled=True),
        lax.all_gather(key_rot, "tp", axis=0, tiled=True),
    )
    query_first = sp_place * group_rows
    query_index = query_first + jnp.arange(group_rows)
    head_count = q_up.shape[1] // (NOPE + ROPE)
    query = jnp.dot(q_group, q_up, preferred_element_type=jnp.float32).reshape(
        group_rows, head_count, NOPE + ROPE
    )
    query = jnp.concatenate(
        [query[..., :NOPE], rotate(query[..., NOPE:], query_index.astype(jnp.float32))], axis=-1
    )
    query = query.astype(jnp.bfloat16)
    query_nope = query[..., :NOPE]
    query_rot = query[..., NOPE:]
    factor = (NOPE + ROPE) ** (-0.5)

    def attend_block(state, key_rows, rot_rows, block_first):

        def compute(state_in):
            top_score, total, summed = state_in
            keys_values = jnp.dot(key_rows, kv_up, preferred_element_type=jnp.float32).astype(
                jnp.bfloat16
            )
            keys_values = keys_values.reshape(key_rows.shape[0], head_count, NOPE + VDIM)
            scores = jnp.einsum(
                "qhd,khd->hqk",
                query_nope,
                keys_values[..., :NOPE],
                preferred_element_type=jnp.float32,
            )
            scores = scores + jnp.einsum(
                "qhd,kd->hqk", query_rot, rot_rows, preferred_element_type=jnp.float32
            )
            scores = scores * factor
            key_index = block_first + jnp.arange(key_rows.shape[0])
            visible = (key_index[None, :] <= query_index[:, None])[None]
            scores = jnp.where(visible, scores, -1e30)
            new_top = jnp.maximum(top_score, jnp.max(scores, axis=-1))
            correction = jnp.exp(top_score - new_top)
            weights = jnp.where(visible, jnp.exp(scores - new_top[..., None]), 0.0)
            total_new = total * correction + jnp.sum(weights, axis=-1)
            product = jnp.einsum(
                "hqk,khd->hqd",
                weights.astype(jnp.bfloat16),
                keys_values[..., NOPE:],
                preferred_element_type=jnp.float32,
            )
            return (new_top, total_new, summed * correction[..., None] + product)

        return lax.cond(
            block_first <= query_first + group_rows - 1, compute, lambda state_in: state_in, state
        )

    start_state = (
        jnp.full((head_count, group_rows), -1e30, jnp.float32),
        jnp.zeros((head_count, group_rows), jnp.float32),
        jnp.zeros((head_count, group_rows, VDIM), jnp.float32),
    )
    key_piece = lax.all_gather(kv_group, "sp", axis=0, tiled=True)
    rot_piece = lax.all_gather(rot_group, "sp", axis=0, tiled=True)
    piece_rows = rot_piece.shape[0]
    block_count = piece_rows // group_rows
    key_blocks = key_piece.reshape((block_count, group_rows) + key_piece.shape[1:])
    rot_blocks = rot_piece.reshape(block_count, group_rows, rot_piece.shape[1])

    def step(state_in, index):
        block_first = index * group_rows
        return (attend_block(state_in, key_blocks[index], rot_blocks[index], block_first), None)

    state_out, unused = lax.scan(step, start_state, jnp.arange(block_count))
    top_score, total, summed = state_out
    attended = (summed / total[..., None]).transpose(1, 0, 2).reshape(group_rows, head_count * VDIM)
    attended = attended.astype(jnp.bfloat16)
    own_heads = lax.all_to_all(attended, "tp", split_axis=0, concat_axis=1, tiled=True)
    projected = jnp.dot(own_heads, out_weight, preferred_element_type=jnp.float32)
    return scaled_norm(projected, out_gain).astype(jnp.bfloat16)


def solution(mesh):
    return jax.shard_map(
        local,
        mesh=mesh,
        in_specs=(
            P(("sp", "tp"), None),
            P(),
            P(),
            P(),
            P(),
            P(),
            P(),
            P(None, "tp"),
            P(None, "tp"),
            P(),
            P(),
        ),
        out_specs=P(("sp", "tp"), None),
        check_vma=False,
    )
```

profile of v0, /device:TPU:26, one launch (start us, length us, event | category | flops | bytes accessed | tf_op | source)
XLA Modules:
  0.0 503.1 jit_solution(1699244683318475322)
XLA Ops:
  19.8 12.0 %all-gather.4.cloned.1.call-done = bf16[1024,512]{1,0:T(8,128)(2,1)} async-done(((bf16[256,512]{1,0:T(8,128)(2,1)}), bf16[1024,512]{1,0:T(8,128)(2,1)}) %all-gather.4.cloned.1.call-update) | async-done | bytes 1048592 | tf_op jit(solution)/shard_map/all_gather | solution.py:67
  38.0 32.3 %all_gather.19 = bf16[8192,32]{0,1:T(8,128)(2,1)S(1)} all-gather(bf16[1024,32]{0,1:T(8,128)(2,1)S(1)} %all_gather.18), channel_id=1, replica_groups=mesh['sp'=8,'tp'=4] {'sp'}, dimensions={0}, use_global_device_ids=true | all-gather | bytes 589824 | tf_op jit(solution)/shard_map/all_gather | solution.py:127
  73.9 102.8 %all-gather.6.cloned.1.call-done = bf16[8192,512]{1,0:T(8,128)(2,1)} async-done(((bf16[1024,512]{1,0:T(8,128)(2,1)}), bf16[8192,512]{1,0:T(8,128)(2,1)}) %all-gather.6.cloned.1.call-update) | async-done | bytes 8388624 | tf_op jit(solution)/shard_map/all_gather | solution.py:126
  177.9 297.7 %while.17 = (s32[]{:T(128)}, f32[4,1024]{1,0:T(4,128)S(1)}, f32[4,1024]{1,0:T(4,128)S(1)}, f32[4,1024,64]{1,2,0:T(8,128)}, s32[8]{0:T(128)S(1)}, /*index=5*/s32[...) while((s32[]{:T(128)}, f32[4,1024]{1,0:T(4,128)S(1)}, ...), condition=%wide.region_8.9_spmd.clone, body=%wide.region_3.8_spmd.clone.sunk | while | flops 1923098624 | bytes 107569616 | solution.py:137
  179.0 36.1 %conditional.3 = ((f32[4,1024]{1,0:T(4,128)S(1)}, f32[4,1024]{1,0:T(4,128)S(1)}, f32[4,1024,64]{1,2,0:T(8,128)})) conditional(s32[]{:T(128)} %convert_element_type.106, (f32[4,1024]{1,0:T(4,128)S(1)}, f32[4,1024]{1,0:T(4,128)S(1)}, f32[4,1024,64]{1,2,0:T(8,128)}) %tuple.62, (s32[]{:T(128)}, s32[]{:T(128)}, s32[]{:T(128)}, ...), branch_computations={%region_4.4_spmd, %region_5.7_spmd} | conditional | flops 1923098624 | bytes 107565224 | solution.py:117
  187.9 9.2 %fusion.40 = (f32[4,1024]{1,0:T(4,128)S(1)}, f32[4,1024,1024]{1,2,0:T(8,128)}) fusion(bf16[1024,4,32]{0,2,1:T(8,128)(2,1)S(1)} %get-tuple-element.258, bf16[8,1024,32]{1,2,0:T(8,128)(2,1)} %get-tuple-element.257, s32[]{:T(128)S(6)} %select_n.18, f32[4,1024,1024]{2,1,0:T(8,128)S(1)} %fusion.15, pred[1024,1024]{0,1:T(8,128)(4,1)} %broadcast_compare_fusion), kind=kOutput, calls=%fused_computation.67 | convolution fusion | flops 285208576 | bytes 34947076 | tf_op jit(solution)/shard_map/while/body/eval_jaxpr/cond/branch_1_fun/qhd,kd->hqk/dot_general | solution.py:98
  197.1 9.2 %fusion.5 = f32[4,1024]{1,0:T(4,128)S(1)} fusion(f32[4,1024,1024]{1,2,0:T(8,128)} %get-tuple-element.389, f32[4,1024]{1,0:T(4,128)S(1)} %max.5, pred[1024,1024]{0,1:T(8,128)(4,1)} %broadcast_compare_fusion), kind=kLoop, calls=%fused_computation.6 | loop fusion | flops 12578816 | bytes 17858560 | tf_op jit(solution)/shard_map/while/body/eval_jaxpr/cond/branch_1_fun/reduce_sum | solution.py:108
  216.2 36.1 %conditional.3 = ((f32[4,1024]{1,0:T(4,128)S(1)}, f32[4,1024]{1,0:T(4,128)S(1)}, f32[4,1024,64]{1,2,0:T(8,128)})) conditional(s32[]{:T(128)} %convert_element_type.106, (f32[4,1024]{1,0:T(4,128)S(1)}, f32[4,1024]{1,0:T(4,128)S(1)}, f32[4,1024,64]{1,2,0:T(8,128)}) %tuple.62, (s32[]{:T(128)}, s32[]{:T(128)}, s32[]{:T(128)}, ...), branch_computations={%region_4.4_spmd, %region_5.7_spmd} | conditional | flops 1923098624 | bytes 107565224 | solution.py:117
  225.2 9.2 %fusion.40 = (f32[4,1024]{1,0:T(4,128)S(1)}, f32[4,1024,1024]{1,2,0:T(8,128)}) fusion(bf16[1024,4,32]{0,2,1:T(8,128)(2,1)S(1)} %get-tuple-element.258, bf16[8,1024,32]{1,2,0:T(8,128)(2,1)} %get-tuple-element.257, s32[]{:T(128)S(6)} %select_n.18, f32[4,1024,1024]{2,1,0:T(8,128)S(1)} %fusion.15, pred[1024,1024]{0,1:T(8,128)(4,1)} %broadcast_compare_fusion), kind=kOutput, calls=%fused_computation.67 | convolution fusion | flops 285208576 | bytes 34947076 | tf_op jit(solution)/shard_map/while/body/eval_jaxpr/cond/branch_1_fun/qhd,kd->hqk/dot_general | solution.py:98
  234.3 9.2 %fusion.5 = f32[4,1024]{1,0:T(4,128)S(1)} fusion(f32[4,1024,1024]{1,2,0:T(8,128)} %get-tuple-element.389, f32[4,1024]{1,0:T(4,128)S(1)} %max.5, pred[1024,1024]{0,1:T(8,128)(4,1)} %broadcast_compare_fusion), kind=kLoop, calls=%fused_computation.6 | loop fusion | flops 12578816 | bytes 17858560 | tf_op jit(solution)/shard_map/while/body/eval_jaxpr/cond/branch_1_fun/reduce_sum | solution.py:108
  253.5 36.1 %conditional.3 = ((f32[4,1024]{1,0:T(4,128)S(1)}, f32[4,1024]{1,0:T(4,128)S(1)}, f32[4,1024,64]{1,2,0:T(8,128)})) conditional(s32[]{:T(128)} %convert_element_type.106, (f32[4,1024]{1,0:T(4,128)S(1)}, f32[4,1024]{1,0:T(4,128)S(1)}, f32[4,1024,64]{1,2,0:T(8,128)}) %tuple.62, (s32[]{:T(128)}, s32[]{:T(128)}, s32[]{:T(128)}, ...), branch_computations={%region_4.4_spmd, %region_5.7_spmd} | conditional | flops 1923098624 | bytes 107565224 | solution.py:117
  262.4 9.2 %fusion.40 = (f32[4,1024]{1,0:T(4,128)S(1)}, f32[4,1024,1024]{1,2,0:T(8,128)}) fusion(bf16[1024,4,32]{0,2,1:T(8,128)(2,1)S(1)} %get-tuple-element.258, bf16[8,1024,32]{1,2,0:T(8,128)(2,1)} %get-tuple-element.257, s32[]{:T(128)S(6)} %select_n.18, f32[4,1024,1024]{2,1,0:T(8,128)S(1)} %fusion.15, pred[1024,1024]{0,1:T(8,128)(4,1)} %broadcast_compare_fusion), kind=kOutput, calls=%fused_computation.67 | convolution fusion | flops 285208576 | bytes 34947076 | tf_op jit(solution)/shard_map/while/body/eval_jaxpr/cond/branch_1_fun/qhd,kd->hqk/dot_general | solution.py:98
  290.7 36.1 %conditional.3 = ((f32[4,1024]{1,0:T(4,128)S(1)}, f32[4,1024]{1,0:T(4,128)S(1)}, f32[4,1024,64]{1,2,0:T(8,128)})) conditional(s32[]{:T(128)} %convert_element_type.106, (f32[4,1024]{1,0:T(4,128)S(1)}, f32[4,1024]{1,0:T(4,128)S(1)}, f32[4,1024,64]{1,2,0:T(8,128)}) %tuple.62, (s32[]{:T(128)}, s32[]{:T(128)}, s32[]{:T(128)}, ...), branch_computations={%region_4.4_spmd, %region_5.7_spmd} | conditional | flops 1923098624 | bytes 107565224 | solution.py:117
  299.6 9.2 %fusion.40 = (f32[4,1024]{1,0:T(4,128)S(1)}, f32[4,1024,1024]{1,2,0:T(8,128)}) fusion(bf16[1024,4,32]{0,2,1:T(8,128)(2,1)S(1)} %get-tuple-element.258, bf16[8,1024,32]{1,2,0:T(8,128)(2,1)} %get-tuple-element.257, s32[]{:T(128)S(6)} %select_n.18, f32[4,1024,1024]{2,1,0:T(8,128)S(1)} %fusion.15, pred[1024,1024]{0,1:T(8,128)(4,1)} %broadcast_compare_fusion), kind=kOutput, calls=%fused_computation.67 | convolution fusion | flops 285208576 | bytes 34947076 | tf_op jit(solution)/shard_map/while/body/eval_jaxpr/cond/branch_1_fun/qhd,kd->hqk/dot_general | solution.py:98
  327.9 36.1 %conditional.3 = ((f32[4,1024]{1,0:T(4,128)S(1)}, f32[4,1024]{1,0:T(4,128)S(1)}, f32[4,1024,64]{1,2,0:T(8,128)})) conditional(s32[]{:T(128)} %convert_element_type.106, (f32[4,1024]{1,0:T(4,128)S(1)}, f32[4,1024]{1,0:T(4,128)S(1)}, f32[4,1024,64]{1,2,0:T(8,128)}) %tuple.62, (s32[]{:T(128)}, s32[]{:T(128)}, s32[]{:T(128)}, ...), branch_computations={%region_4.4_spmd, %region_5.7_spmd} | conditional | flops 1923098624 | bytes 107565224 | solution.py:117
  336.8 9.2 %fusion.40 = (f32[4,1024]{1,0:T(4,128)S(1)}, f32[4,1024,1024]{1,2,0:T(8,128)}) fusion(bf16[1024,4,32]{0,2,1:T(8,128)(2,1)S(1)} %get-tuple-element.258, bf16[8,1024,32]{1,2,0:T(8,128)(2,1)} %get-tuple-element.257, s32[]{:T(128)S(6)} %select_n.18, f32[4,1024,1024]{2,1,0:T(8,128)S(1)} %fusion.15, pred[1024,1024]{0,1:T(8,128)(4,1)} %broadcast_compare_fusion), kind=kOutput, calls=%fused_computation.67 | convolution fusion | flops 285208576 | bytes 34947076 | tf_op jit(solution)/shard_map/while/body/eval_jaxpr/cond/branch_1_fun/qhd,kd->hqk/dot_general | solution.py:98
  365.1 36.1 %conditional.3 = ((f32[4,1024]{1,0:T(4,128)S(1)}, f32[4,1024]{1,0:T(4,128)S(1)}, f32[4,1024,64]{1,2,0:T(8,128)})) conditional(s32[]{:T(128)} %convert_element_type.106, (f32[4,1024]{1,0:T(4,128)S(1)}, f32[4,1024]{1,0:T(4,128)S(1)}, f32[4,1024,64]{1,2,0:T(8,128)}) %tuple.62, (s32[]{:T(128)}, s32[]{:T(128)}, s32[]{:T(128)}, ...), branch_computations={%region_4.4_spmd, %region_5.7_spmd} | conditional | flops 1923098624 | bytes 107565224 | solution.py:117
  374.0 9.2 %fusion.40 = (f32[4,1024]{1,0:T(4,128)S(1)}, f32[4,1024,1024]{1,2,0:T(8,128)}) fusion(bf16[1024,4,32]{0,2,1:T(8,128)(2,1)S(1)} %get-tuple-element.258, bf16[8,1024,32]{1,2,0:T(8,128)(2,1)} %get-tuple-element.257, s32[]{:T(128)S(6)} %select_n.18, f32[4,1024,1024]{2,1,0:T(8,128)S(1)} %fusion.15, pred[1024,1024]{0,1:T(8,128)(4,1)} %broadcast_compare_fusion), kind=kOutput, calls=%fused_computation.67 | convolution fusion | flops 285208576 | bytes 34947076 | tf_op jit(solution)/shard_map/while/body/eval_jaxpr/cond/branch_1_fun/qhd,kd->hqk/dot_general | solution.py:98
  402.3 36.1 %conditional.3 = ((f32[4,1024]{1,0:T(4,128)S(1)}, f32[4,1024]{1,0:T(4,128)S(1)}, f32[4,1024,64]{1,2,0:T(8,128)})) conditional(s32[]{:T(128)} %convert_element_type.106, (f32[4,1024]{1,0:T(4,128)S(1)}, f32[4,1024]{1,0:T(4,128)S(1)}, f32[4,1024,64]{1,2,0:T(8,128)}) %tuple.62, (s32[]{:T(128)}, s32[]{:T(128)}, s32[]{:T(128)}, ...), branch_computations={%region_4.4_spmd, %region_5.7_spmd} | conditional | flops 1923098624 | bytes 107565224 | solution.py:117
  411.2 9.2 %fusion.40 = (f32[4,1024]{1,0:T(4,128)S(1)}, f32[4,1024,1024]{1,2,0:T(8,128)}) fusion(bf16[1024,4,32]{0,2,1:T(8,128)(2,1)S(1)} %get-tuple-element.258, bf16[8,1024,32]{1,2,0:T(8,128)(2,1)} %get-tuple-element.257, s32[]{:T(128)S(6)} %select_n.18, f32[4,1024,1024]{2,1,0:T(8,128)S(1)} %fusion.15, pred[1024,1024]{0,1:T(8,128)(4,1)} %broadcast_compare_fusion), kind=kOutput, calls=%fused_computation.67 | convolution fusion | flops 285208576 | bytes 34947076 | tf_op jit(solution)/shard_map/while/body/eval_jaxpr/cond/branch_1_fun/qhd,kd->hqk/dot_general | solution.py:98
  420.4 9.2 %fusion.5 = f32[4,1024]{1,0:T(4,128)S(1)} fusion(f32[4,1024,1024]{1,2,0:T(8,128)} %get-tuple-element.389, f32[4,1024]{1,0:T(4,128)S(1)} %max.5, pred[1024,1024]{0,1:T(8,128)(4,1)} %broadcast_compare_fusion), kind=kLoop, calls=%fused_computation.6 | loop fusion | flops 12578816 | bytes 17858560 | tf_op jit(solution)/shard_map/while/body/eval_jaxpr/cond/branch_1_fun/reduce_sum | solution.py:108
  439.5 36.1 %conditional.3 = ((f32[4,1024]{1,0:T(4,128)S(1)}, f32[4,1024]{1,0:T(4,128)S(1)}, f32[4,1024,64]{1,2,0:T(8,128)})) conditional(s32[]{:T(128)} %convert_element_type.106, (f32[4,1024]{1,0:T(4,128)S(1)}, f32[4,1024]{1,0:T(4,128)S(1)}, f32[4,1024,64]{1,2,0:T(8,128)}) %tuple.62, (s32[]{:T(128)}, s32[]{:T(128)}, s32[]{:T(128)}, ...), branch_computations={%region_4.4_spmd, %region_5.7_spmd} | conditional | flops 1923098624 | bytes 107565224 | solution.py:117
  448.4 9.2 %fusion.40 = (f32[4,1024]{1,0:T(4,128)S(1)}, f32[4,1024,1024]{1,2,0:T(8,128)}) fusion(bf16[1024,4,32]{0,2,1:T(8,128)(2,1)S(1)} %get-tuple-element.258, bf16[8,1024,32]{1,2,0:T(8,128)(2,1)} %get-tuple-element.257, s32[]{:T(128)S(6)} %select_n.18, f32[4,1024,1024]{2,1,0:T(8,128)S(1)} %fusion.15, pred[1024,1024]{0,1:T(8,128)(4,1)} %broadcast_compare_fusion), kind=kOutput, calls=%fused_computation.67 | convolution fusion | flops 285208576 | bytes 34947076 | tf_op jit(solution)/shard_map/while/body/eval_jaxpr/cond/branch_1_fun/qhd,kd->hqk/dot_general | solution.py:98
  477.4 11.4 %all_to_all.16 = bf16[4,256,256]{1,2,0:T(8,128)(2,1)S(1)} all-to-all(bf16[4,256,256]{1,2,0:T(8,128)(2,1)S(1)} %copy.21), channel_id=1, replica_groups=mesh['sp'=8,'tp'=4] {'tp'}, dimensions={0} | all-to-all | bytes 1048576 | tf_op jit(solution)/shard_map/all_to_all | solution.py:141
  (187 shorter events, 211.7 us)
Async XLA Ops:
  6.5 65.0 %copy-start = (bf16[768,384]{1,0:T(8,128)(2,1)S(1)}, bf16[768,384]{1,0:T(8,128)(2,1)}, u32[]{:S(2)}) copy-start(bf16[768,384]{1,0:T(8,128)(2,1)} %param.22) | copy-start | bytes 1769476
  6.5 25.2 %all-gather.4.cloned.1.call-start = ((), (), s32[]{:S(2)}) async-start(), calls=%async_computation.1 | async-start | bytes 1310720 | tf_op jit(solution)/shard_map/all_gather | solution.py:67
  8.7 5.3 %copy-start.5 = (bf16[256,4096]{1,0:T(8,128)(2,1)S(1)}, bf16[256,4096]{1,0:T(8,128)(2,1)}, u32[]{:S(2)}) copy-start(bf16[256,4096]{1,0:T(8,128)(2,1)} %param.15) | copy-start | bytes 6291460
  14.0 17.9 %copy-start.9 = (bf16[4096,32]{0,1:T(8,128)(2,1)S(1)}, bf16[4096,32]{0,1:T(8,128)(2,1)}, u32[]{:S(2)}) copy-start(bf16[4096,32]{0,1:T(8,128)(2,1)} %param.19) | copy-start | bytes 786436
  14.0 57.5 %all-gather.8.cloned.1.call-start = ((), (), s32[]{:S(2)}) async-start(), calls=%async_computation.3 | async-start | bytes 1966080 | tf_op jit(solution)/shard_map/all_gather | solution.py:66
  19.7 157.1 %all-gather.6.cloned.1.call-start = ((), (), s32[]{:S(2)}) async-start(), calls=%async_computation.2 | async-start | bytes 9437184 | tf_op jit(solution)/shard_map/all_gather | solution.py:126
  197.1 9.2 %copy-start.2 = (pred[1024,1024]{0,1:T(8,128)(4,1)S(1)}, pred[1024,1024]{0,1:T(8,128)(4,1)}, u32[]{:S(2)}) copy-start(pred[1024,1024]{0,1:T(8,128)(4,1)} %broadcast_compare_fusion) | copy-start | bytes 3145732 | tf_op jit(solution)/shard_map/while/body/eval_jaxpr/cond
  197.1 9.2 %copy-start.4 = (bf16[1024,512]{0,1:T(8,128)(2,1)S(1)}, bf16[1024,512]{0,1:T(8,128)(2,1)}, u32[]{:S(2)}) copy-start(bf16[1024,512]{0,1:T(8,128)(2,1)} %copy-done.3) | copy-start | bytes 3145732 | tf_op jit(solution)/shard_map/while/body/eval_jaxpr/cond
  234.3 9.2 %copy-start.2 = (pred[1024,1024]{0,1:T(8,128)(4,1)S(1)}, pred[1024,1024]{0,1:T(8,128)(4,1)}, u32[]{:S(2)}) copy-start(pred[1024,1024]{0,1:T(8,128)(4,1)} %broadcast_compare_fusion) | copy-start | bytes 3145732 | tf_op jit(solution)/shard_map/while/body/eval_jaxpr/cond
  234.3 9.2 %copy-start.4 = (bf16[1024,512]{0,1:T(8,128)(2,1)S(1)}, bf16[1024,512]{0,1:T(8,128)(2,1)}, u32[]{:S(2)}) copy-start(bf16[1024,512]{0,1:T(8,128)(2,1)} %copy-done.3) | copy-start | bytes 3145732 | tf_op jit(solution)/shard_map/while/body/eval_jaxpr/cond
  271.5 9.2 %copy-start.2 = (pred[1024,1024]{0,1:T(8,128)(4,1)S(1)}, pred[1024,1024]{0,1:T(8,128)(4,1)}, u32[]{:S(2)}) copy-start(pred[1024,1024]{0,1:T(8,128)(4,1)} %broadcast_compare_fusion) | copy-start | bytes 3145732 | tf_op jit(solution)/shard_map/while/body/eval_jaxpr/cond
  271.5 9.2 %copy-start.4 = (bf16[1024,512]{0,1:T(8,128)(2,1)S(1)}, bf16[1024,512]{0,1:T(8,128)(2,1)}, u32[]{:S(2)}) copy-start(bf16[1024,512]{0,1:T(8,128)(2,1)} %copy-done.3) | copy-start | bytes 3145732 | tf_op jit(solution)/shard_map/while/body/eval_jaxpr/cond
  308.7 9.2 %copy-start.2 = (pred[1024,1024]{0,1:T(8,128)(4,1)S(1)}, pred[1024,1024]{0,1:T(8,128)(4,1)}, u32[]{:S(2)}) copy-start(pred[1024,1024]{0,1:T(8,128)(4,1)} %broadcast_compare_fusion) | copy-start | bytes 3145732 | tf_op jit(solution)/shard_map/while/body/eval_jaxpr/cond
  308.8 9.2 %copy-start.4 = (bf16[1024,512]{0,1:T(8,128)(2,1)S(1)}, bf16[1024,512]{0,1:T(8,128)(2,1)}, u32[]{:S(2)}) copy-start(bf16[1024,512]{0,1:T(8,128)(2,1)} %copy-done.3) | copy-start | bytes 3145732 | tf_op jit(solution)/shard_map/while/body/eval_jaxpr/cond
  346.0 9.2 %copy-start.2 = (pred[1024,1024]{0,1:T(8,128)(4,1)S(1)}, pred[1024,1024]{0,1:T(8,128)(4,1)}, u32[]{:S(2)}) copy-start(pred[1024,1024]{0,1:T(8,128)(4,1)} %broadcast_compare_fusion) | copy-start | bytes 3145732 | tf_op jit(solution)/shard_map/while/body/eval_jaxpr/cond
  346.0 9.2 %copy-start.4 = (bf16[1024,512]{0,1:T(8,128)(2,1)S(1)}, bf16[1024,512]{0,1:T(8,128)(2,1)}, u32[]{:S(2)}) copy-start(bf16[1024,512]{0,1:T(8,128)(2,1)} %copy-done.3) | copy-start | bytes 3145732 | tf_op jit(solution)/shard_map/while/body/eval_jaxpr/cond
  383.2 9.2 %copy-start.2 = (pred[1024,1024]{0,1:T(8,128)(4,1)S(1)}, pred[1024,1024]{0,1:T(8,128)(4,1)}, u32[]{:S(2)}) copy-start(pred[1024,1024]{0,1:T(8,128)(4,1)} %broadcast_compare_fusion) | copy-start | bytes 3145732 | tf_op jit(solution)/shard_map/while/body/eval_jaxpr/cond
  383.2 9.2 %copy-start.4 = (bf16[1024,512]{0,1:T(8,128)(2,1)S(1)}, bf16[1024,512]{0,1:T(8,128)(2,1)}, u32[]{:S(2)}) copy-start(bf16[1024,512]{0,1:T(8,128)(2,1)} %copy-done.3) | copy-start | bytes 3145732 | tf_op jit(solution)/shard_map/while/body/eval_jaxpr/cond
  420.4 9.2 %copy-start.2 = (pred[1024,1024]{0,1:T(8,128)(4,1)S(1)}, pred[1024,1024]{0,1:T(8,128)(4,1)}, u32[]{:S(2)}) copy-start(pred[1024,1024]{0,1:T(8,128)(4,1)} %broadcast_compare_fusion) | copy-start | bytes 3145732 | tf_op jit(solution)/shard_map/while/body/eval_jaxpr/cond
  420.4 9.2 %copy-start.4 = (bf16[1024,512]{0,1:T(8,128)(2,1)S(1)}, bf16[1024,512]{0,1:T(8,128)(2,1)}, u32[]{:S(2)}) copy-start(bf16[1024,512]{0,1:T(8,128)(2,1)} %copy-done.3) | copy-start | bytes 3145732 | tf_op jit(solution)/shard_map/while/body/eval_jaxpr/cond
  457.6 9.2 %copy-start.2 = (pred[1024,1024]{0,1:T(8,128)(4,1)S(1)}, pred[1024,1024]{0,1:T(8,128)(4,1)}, u32[]{:S(2)}) copy-start(pred[1024,1024]{0,1:T(8,128)(4,1)} %broadcast_compare_fusion) | copy-start | bytes 3145732 | tf_op jit(solution)/shard_map/while/body/eval_jaxpr/cond
  457.6 9.2 %copy-start.4 = (bf16[1024,512]{0,1:T(8,128)(2,1)S(1)}, bf16[1024,512]{0,1:T(8,128)(2,1)}, u32[]{:S(2)}) copy-start(bf16[1024,512]{0,1:T(8,128)(2,1)} %copy-done.3) | copy-start | bytes 3145732 | tf_op jit(solution)/shard_map/while/body/eval_jaxpr/cond
  488.7 6.0 %copy-start.6 = (f32[4096]{0:T(1024)S(1)}, f32[4096]{0:T(1024)}, u32[]{:S(2)}) copy-start(f32[4096]{0:T(1024)} %param.25) | copy-start | bytes 49156
  488.7 7.9 %copy-start.1 = (bf16[768,384]{1,0:T(8,128)(2,1)S(1)}, bf16[768,384]{1,0:T(8,128)(2,1)}, u32[]{:S(2)}) copy-start(bf16[768,384]{1,0:T(8,128)(2,1)} %param.22) | copy-start | bytes 1769476
  (11 other events, 22.3 us)
Sparse Core Ops, SparseCore 0:
  14.1 17.6 all-gather.3
  33.3 19.6 all-gather.7
  55.1 121.5 all-gather.5
where the time goes:
time: 504 us; the launch traced here: 503 us
  matrix products  197 us (39%)
  waiting for transfers between devices  115 us (23%)
  other arithmetic  94.9 us (19%)
  blocking collectives  48.9 us (10%)
  loops' own time  18.9 us (4%)
  local copies, waits for them, and re-layouts  14.8 us (3%)
  between operations  13.3 us (3%)
    all_gather x1, waiting for transfers between devices, local(): key_piece = lax.all_gather(kv_group, 'sp', axis=0, tiled=True)  103 us
    dot_general x8, matrix products, compute(): jnp.einsum('qhd,kd->hqk', query_rot, rot_rows, preferred_element_type=jnp...  73.2 us
    reduce_sum x8, other arithmetic, compute(): total_new = total * correction + jnp.sum(weights, axis=-1)  73.2 us
    dot_general x8, matrix products, compute(): jnp.einsum('hqk,khd->hqd', weights.astype(jnp.bfloat16), keys_values[...,...  70.1 us
    all_gather x1, blocking collectives, local(): rot_piece = lax.all_gather(rot_group, 'sp', axis=0, tiled=True)  32.3 us
    dot_general x8, matrix products, compute(): jnp.einsum('qhd,khd->hqk', query_nope, keys_values[..., :NOPE], preferred...  19 us
    dot_general x8, matrix products, compute(): jnp.dot(key_rows, kv_up, preferred_element_type=jnp.float32)  16.8 us
    another operation x8, loops' own time, attend_block(): lax.cond(block_first <= query_first + group_rows - 1, compute, lambda sta...  14.3 us
  transfers between devices with their start and end apart: 3, of which 2 were waited for; matrix products, arithmetic and copies ran while one was open for 2% of the time, Pallas kernels for 0%

commit v1 on v0

v1 whole, which is shorter than its diff:
```python
import functools

import jax
import jax.numpy as jnp
from jax import lax
from jax.experimental import pallas as pl
from jax.experimental.pallas import tpu as pltpu
from jax.sharding import PartitionSpec as P

NOPE = 64
ROPE = 32
VDIM = 64
HEAD_KV = NOPE + VDIM

EPS = 1e-06
THETA = 500000.0
LOG2E = 1.4426950408889634
FLOOR = -1e30
Q_TILE = 256
K_TILE = 512
V_ROWS = VDIM + 16


def scaled_norm(values_in, gain):
    values_in = values_in.astype(jnp.float32)
    return (
        values_in * lax.rsqrt(jnp.mean(values_in * values_in, axis=-1, keepdims=True) + EPS) * gain
    )


def angle_tables(position):
    inverse = 1.0 / THETA ** (jnp.arange(0, ROPE, 2, dtype=jnp.float32) / ROPE)
    return position.astype(jnp.float32)[:, None] * inverse[None, :]


def rotate(values_in, position):
    angles = angle_tables(position)
    cosine = jnp.cos(angles)
    sine = jnp.sin(angles)
    left = values_in[:, : ROPE // 2]
    right = values_in[:, ROPE // 2 :]
    return jnp.concatenate([left * cosine - right * sine, right * cosine + left * sine], axis=-1)


def attend_kernel(
    rows,
    heads,
    group_rows,
    rank,
    place_ref,
    q_lat_ref,
    q_up_ref,
    cos_ref,
    sin_ref,
    position_ref,
    lat_ref,
    kv_up_ref,
    v_up_ref,
    out_ref,
    query_ref,
    key_ref,
    value_ref,
    sum_ref,
    top_ref,
):
    chunk = pl.program_id(0)
    half = rows // 2
    side = group_rows // 2
    width = NOPE + ROPE
    scale = width**-0.5 * LOG2E

    @pl.when(chunk == 0)
    def _():
        cosine = cos_ref[...]
        sine = sin_ref[...]
        middle = NOPE + ROPE // 2
        for head in range(heads):
            turned = lax.dot_general(
                q_up_ref[head],
                q_lat_ref[...],
                (((1,), (1,)), ((), ())),
                preferred_element_type=jnp.float32,
            )
            left = turned[NOPE:middle]
            right = turned[middle:]
            query_ref[head, :NOPE] = turned[:NOPE].astype(jnp.bfloat16)
            query_ref[head, NOPE:middle] = (left * cosine - right * sine).astype(jnp.bfloat16)
            query_ref[head, middle:width] = (right * cosine + left * sine).astype(jnp.bfloat16)
            query_ref[head, width:] = jnp.zeros((128 - width, group_rows), jnp.bfloat16)
            row = lax.broadcasted_iota(jnp.int32, (16, group_rows), 0)
            value_ref[head, VDIM:] = jnp.where(row == 0, 1.0, 0.0).astype(jnp.bfloat16)
            sum_ref[head] = jnp.zeros((V_ROWS, group_rows), jnp.float32)
            top_ref[head] = jnp.full((1, group_rows), FLOOR, jnp.float32)

    own = place_ref[0]
    mate = place_ref[1]

    @pl.when(chunk <= jnp.maximum(own, mate))
    def _():
        lat = lat_ref[:, :rank]
        turned = lat_ref[:, rank:]
        lane = lax.broadcasted_iota(jnp.int32, (group_rows, HEAD_KV), 1)
        for head in range(heads):
            raw = jnp.dot(
                lat,
                kv_up_ref[:, head * HEAD_KV : (head + 1) * HEAD_KV],
                preferred_element_type=jnp.float32,
            ).astype(jnp.bfloat16)
            key_ref[head] = jnp.where(lane < NOPE, raw, turned)
        values = lax.dot_general(
            v_up_ref[...], lat, (((1,), (1,)), ((), ())), preferred_element_type=jnp.float32
        ).astype(jnp.bfloat16)
        for head in range(heads):
            value_ref[head, :VDIM] = values[head * VDIM : (head + 1) * VDIM]

        key_steps = group_rows // K_TILE
        query_steps = group_rows // Q_TILE

        def pair(masked, column, key_row):
            columns = pl.ds(column, Q_TILE)
            keys = pl.ds(key_row, K_TILE)
            if masked:
                key_index = (
                    chunk * group_rows
                    + key_row
                    + lax.broadcasted_iota(jnp.int32, (K_TILE, Q_TILE), 0)
                )
                visible = key_index <= position_ref[:, columns]
            for head in range(heads):
                scores = jnp.dot(
                    key_ref[head, keys, :],
                    query_ref[head, :, columns],
                    preferred_element_type=jnp.float32,
                )
                if masked:
                    scores = jnp.where(visible, scores, FLOOR)
                old = top_ref[head, :, columns]
                new = jnp.maximum(old, jnp.max(scores, axis=0, keepdims=True))
                weights = jnp.exp2((scores - new) * scale)
                product = jnp.dot(
                    value_ref[head, :, keys],
                    weights.astype(jnp.bfloat16),
                    preferred_element_type=jnp.float32,
                )
                sum_ref[head, :, columns] = (
                    sum_ref[head, :, columns] * jnp.exp2((old - new) * scale) + product
                )
                top_ref[head, :, columns] = new

        @pl.loop(0, key_steps * query_steps)
        def _(index):
            column = pl.multiple_of(lax.rem(index, query_steps) * Q_TILE, Q_TILE)
            key_row = pl.multiple_of(lax.div(index, query_steps) * K_TILE, K_TILE)
            second = column >= side
            group = jnp.where(second, mate, own)
            inside = column - jnp.where(second, side, 0)
            base = group * group_rows + jnp.where(second, half, 0)
            first_query = base + lax.div(inside, half) * rows + lax.rem(inside, half)
            last = inside + Q_TILE - 1
            last_query = base + lax.div(last, half) * rows + lax.rem(last, half)
            first_key = chunk * group_rows + key_row
            last_key = first_key + K_TILE - 1

            @pl.when(last_key <= first_query)
            def _():
                pair(False, column, key_row)

            @pl.when((last_key > first_query) & (first_key <= last_query))
            def _():
                pair(True, column, key_row)

    @pl.when(chunk == pl.num_programs(0) - 1)
    def _():
        for column in range(0, group_rows, Q_TILE):
            columns = slice(column, column + Q_TILE)
            parts = [
                sum_ref[head, :VDIM, columns] / sum_ref[head, VDIM : VDIM + 1, columns]
                for head in range(heads)
            ]
            out_ref[columns, :] = jnp.concatenate(parts, axis=0).T.astype(jnp.bfloat16)


def attend(place, q_lat, q_up, cosine, sine, position, latents, kv_up, v_up, rows):
    group_rows, q_rank = q_lat.shape
    heads = q_up.shape[0]
    rank = kv_up.shape[0]
    chunks = latents.shape[0] // group_rows

    def whole(*shape):
        return pl.BlockSpec(shape, lambda chunk, place_ref: (0,) * len(shape))

    pairs = latents.shape[0] * group_rows * heads // 2
    return pl.pallas_call(
        functools.partial(attend_kernel, rows, heads, group_rows, rank),
        out_shape=jax.ShapeDtypeStruct((group_rows, heads * VDIM), jnp.bfloat16),
        grid_spec=pltpu.PrefetchScalarGridSpec(
            num_scalar_prefetch=1,
            grid=(chunks,),
            in_specs=[
                whole(group_rows, q_rank),
                whole(heads, NOPE + ROPE, q_rank),
                whole(ROPE // 2, group_rows),
                whole(ROPE // 2, group_rows),
                whole(1, group_rows),
                pl.BlockSpec(
                    (group_rows, latents.shape[1]),
                    lambda chunk, place_ref: (
                        jnp.minimum(chunk, jnp.maximum(place_ref[0], place_ref[1])),
                        0,
                    ),
                ),
                whole(*kv_up.shape),
                whole(*v_up.shape),
            ],
            out_specs=whole(group_rows, heads * VDIM),
            scratch_shapes=[
                pltpu.VMEM((heads, 128, group_rows), jnp.bfloat16),
                pltpu.VMEM((heads, group_rows, HEAD_KV), jnp.bfloat16),
                pltpu.VMEM((heads, V_ROWS, group_rows), jnp.bfloat16),
                pltpu.VMEM((heads, V_ROWS, group_rows), jnp.float32),
                pltpu.VMEM((heads, 1, group_rows), jnp.float32),
            ],
        ),
        compiler_params=pltpu.CompilerParams(
            dimension_semantics=("arbitrary",), vmem_limit_bytes=48 * 1024 * 1024
        ),
        cost_estimate=pl.CostEstimate(
            flops=pairs * 640, bytes_accessed=latents.size * 2, transcendentals=pairs
        ),
    )(place, q_lat, q_up, cosine, sine, position, latents, kv_up, v_up)


def local(
    tokens,
    norm_gain,
    q_down,
    kv_down,
    rope_down,
    q_gain,
    kv_gain,
    q_up,
    kv_up,
    out_weight,
    out_gain,
):
    rows = tokens.shape[0]
    tp_count = lax.axis_size("tp")
    sp_count = lax.axis_size("sp")
    tp_place = lax.axis_index("tp")
    sp_place = lax.axis_index("sp")
    group_rows = rows * tp_count
    half = rows // 2
    row_first = (sp_place * tp_count + tp_place) * rows
    own_position = row_first + jnp.arange(rows)
    heads = q_up.shape[1] // (NOPE + ROPE)
    rank = kv_up.shape[0]

    normed = scaled_norm(tokens, norm_gain).astype(jnp.bfloat16)
    kv_lat = scaled_norm(
        jnp.dot(normed, kv_down, preferred_element_type=jnp.float32), kv_gain
    ).astype(jnp.bfloat16)
    key_rot = rotate(
        jnp.dot(normed, rope_down, preferred_element_type=jnp.float32), own_position
    ).astype(jnp.bfloat16)
    packed = jnp.concatenate(
        [
            kv_lat,
            jnp.zeros((rows, NOPE), jnp.bfloat16),
            key_rot,
            jnp.zeros((rows, 128 - NOPE - ROPE), jnp.bfloat16),
        ],
        axis=1,
    )
    latents = lax.all_gather(packed, ("sp", "tp"), axis=0, tiled=True)

    q_lat = scaled_norm(jnp.dot(normed, q_down, preferred_element_type=jnp.float32), q_gain).astype(
        jnp.bfloat16
    )
    swap = [(place, sp_count - 1 - place) for place in range(sp_count)]
    other = lax.ppermute(q_lat[half:], "sp", swap)
    q_pair = jnp.concatenate([q_lat[:half], other], axis=0)
    q_group = lax.all_gather(q_pair, "tp", axis=0, tiled=True)
    q_group = (
        q_group.reshape(tp_count, 2, half, -1).transpose(1, 0, 2, 3).reshape(group_rows, -1)
    )
    mate = sp_count - 1 - sp_place
    base = jnp.stack([sp_place * group_rows, mate * group_rows + half])
    position = (
        base[:, None, None]
        + (jnp.arange(tp_count) * rows)[None, :, None]
        + jnp.arange(half)[None, None, :]
    ).reshape(group_rows)
    angles = angle_tables(position).T

    q_up_turned = q_up.reshape(-1, heads, NOPE + ROPE).transpose(1, 2, 0)
    v_up = kv_up.reshape(rank, heads, HEAD_KV)[:, :, NOPE:].transpose(1, 2, 0)
    attended = attend(
        jnp.stack([sp_place, mate]).astype(jnp.int32),
        q_group,
        q_up_turned,
        jnp.cos(angles),
        jnp.sin(angles),
        position.astype(jnp.int32)[None, :],
        latents,
        kv_up,
        v_up.reshape(heads * VDIM, rank),
        rows,
    )
    own_heads = lax.all_to_all(
        attended.reshape(2, tp_count, half, heads * VDIM),
        "tp",
        split_axis=1,
        concat_axis=3,
        tiled=True,
    )
    returned = lax.ppermute(own_heads[1, 0], "sp", swap)
    own_rows = jnp.concatenate([own_heads[0, 0], returned], axis=0)
    projected = jnp.dot(own_rows, out_weight, preferred_element_type=jnp.float32)
    return scaled_norm(projected, out_gain).astype(jnp.bfloat16)


def solution(mesh):
    return jax.shard_map(
        local,
        mesh=mesh,
        in_specs=(
            P(("sp", "tp"), None),
            P(),
            P(),
            P(),
            P(),
            P(),
            P(),
            P(None, "tp"),
            P(None, "tp"),
            P(),
            P(),
        ),
        out_specs=P(("sp", "tp"), None),
        check_vma=False,
    )
```

time: 504 us -> 251 us (0.50)
  the two profiles are of different devices: /device:TPU:26 before, /device:TPU:0 now
where the time goes in v1:
time: 251 us
  waiting for transfers between devices  114 us (45%)
  Pallas kernels  74.6 us (30%)
  matrix products  15.7 us (6%)
  between operations  13.6 us (5%)
  blocking collectives  11.4 us (5%)
  starting transfers between devices  8.54 us (3%)
  other arithmetic  6.92 us (3%)
  local copies, waits for them, and re-layouts  5.84 us (2%)
    all_gather x1, waiting for transfers between devices, local(): latents = lax.all_gather(packed, ('sp', 'tp'), axis=0, tiled=True)  87.5 us
    pallas_call x1, Pallas kernels, attend(): pl.pallas_call(functools.partial(attend_kernel, rows, heads, group_rows,...  74.6 us
    all_gather x1, waiting for transfers between devices, local(): q_group = lax.all_gather(q_pair, 'tp', axis=0, tiled=True)  13.6 us
    all_to_all x1, blocking collectives, local(): lax.all_to_all(attended.reshape(2, tp_count, half, heads * VDIM), 'tp', s...  11.4 us
    ppermute x1, waiting for transfers between devices, local(): returned = lax.ppermute(own_heads[1, 0], 'sp', swap)  8.11 us
    ppermute x1, starting transfers between devices, local(): other = lax.ppermute(q_lat[half:], 'sp', swap)  6.06 us
    dot_general x1, matrix products, local(): jnp.dot(own_rows, out_weight, preferred_element_type=jnp.float32)  5.89 us
    dot_general x1, matrix products, local(): jnp.dot(normed, q_down, preferred_element_type=jnp.float32)  5.51 us
  transfers between devices with their start and end apart: 4, of which 4 were waited for; matrix products, arithmetic and copies ran while one was open for 4% of the time, Pallas kernels for 0%

profile of v1, /device:TPU:0, one launch (start us, length us, event | category | flops | bytes accessed | tf_op | source)
XLA Modules:
  0.0 250.9 jit_solution(3738516056549768538)
XLA Ops:
  6.5 2.1 fusion
  8.7 5.5 %multiply_reduce_fusion.1 = (f32[256]{0:T(256)S(1)}, f32[256,768]{1,0:T(8,128)S(1)}) fusion(bf16[4096,768]{1,0:T(8,128)(2,1)} %param.13, bf16[256,4096]{1,0:T(8,128)(2,1)} %param.11, f32[4096]{0:T(1024)} %param.12, f32[256]{0:T(256)S(1)} %add_rsqrt_fusion.3), kind=kOutput, calls=%fused_computation.8 | convolution fusion | flops 1615200000 | bytes 9193472 | tf_op jit(solution)/shard_map/dot_general | solution.py:276
  14.4 6.1 %collective-permute-start = (bf16[128,768]{1,0:T(8,128)(2,1)S(1)}, bf16[128,768]{1,0:T(8,128)(2,1)S(1)}, u32[]{:S(2)}, u32[]{:S(2)}) collective-permute-start(bf16[128,768]{1,0:T(8,128)(2,1)S(1)} %get-tuple-element.8), channel_id=1, source_target_pairs={{0,28},{4,24},{8,20},{12,16},{16,12},{20,8},{24,4},{28,0},{1,29},{... | collective-permute-start | bytes 589832 | tf_op jit(solution)/shard_map/ppermute | solution.py:280
  20.5 5.0 %collective-permute-done = bf16[128,768]{1,0:T(8,128)(2,1)S(1)} collective-permute-done((bf16[128,768]{1,0:T(8,128)(2,1)S(1)}, bf16[128,768]{1,0:T(8,128)(2,1)S(1)}, u32[]{:S(2)}, u32[]{:S(2)}) %collective-permute-start) | collective-permute-done | bytes 196640 | tf_op jit(solution)/shard_map/ppermute | solution.py:280
  25.5 0.8 pad_maximum_fusion
  26.4 3.6 %multiply_reduce_fusion.2 = (f32[256]{0:T(256)S(1)}, f32[256,512]{1,0:T(8,128)S(1)}) fusion(bf16[4096,512]{1,0:T(8,128)(2,1)} %param.14, bf16[256,4096]{1,0:T(8,128)(2,1)S(1)} %copy-done.4, f32[4096]{0:T(1024)S(1)} %copy-done.9, f32[256]{0:T(256)S(1)} %add_rsqrt_fusion.3), kind=kOutput, calls=%fused_computation.15 | convolution fusion | flops 1078198016 | bytes 6834176 | tf_op jit(solution)/shard_map/dot_general | solution.py:260
  30.0 0.8 fusion.17
  30.8 0.6 fusion.14
  31.5 0.9 concatenate.13
  32.5 0.3 copy.31
  33.0 0.7 slice.34
  34.0 0.9 multiply_sine_fusion.1
  34.9 13.6 %all-gather.3.cloned.1.call-done = bf16[1024,768]{1,0:T(8,128)(2,1)} async-done(((bf16[256,768]{1,0:T(8,128)(2,1)}), bf16[1024,768]{1,0:T(8,128)(2,1)}) %all-gather.3.cloned.1.call-update) | async-done | bytes 1572880 | tf_op jit(solution)/shard_map/all_gather | solution.py:282
  48.6 1.5 copy.30
  50.1 87.5 %all-gather.5.cloned.1.call-done.lat_ref = bf16[8192,640]{1,0:T(8,128)(2,1)} async-done(((bf16[256,640]{1,0:T(8,128)(2,1)}), bf16[8192,640]{1,0:T(8,128)(2,1)}) %all-gather.5.cloned.1.call-update) | async-done | bytes 10485776 | tf_op jit(solution)/shard_map/all_gather | solution.py:274
  137.6 0.9 copy-done.2
  138.6 0.8 copy-done.3
  139.4 74.6 %shard_map.109 = bf16[1024,256]{1,0:T(8,128)(2,1)S(1)} custom-call(s32[2]{0:T(128)S(1)} %pad_add_fusion.place_ref, bf16[1024,768]{1,0:T(8,128)(2,1)S(1)} %bitcast.29, bf16[4,96,768]{2,1,0:T(8,128)(2,1)S(1)} %bitcast.30, f32[16,1024]{1,0:T(8,128)S(1)} %copy-done.3, f32[16,1024]{1,0:T(8,128)S(1)} %get-tuple-element.11.sin_ref, s32[1,1024]{1,0:T(1,128)S(1)} %bitcast.33, ...), custom_call_target="tpu_custom_call" | custom-call | flops 10737418240 | bytes 10485760 | tf_op jit(solution)/shard_map/pallas_call | solution.py:193
  214.0 0.3 copy.36
  214.2 11.4 %all_to_all.15 = bf16[2,4,128,256]{2,3,0,1:T(8,128)(2,1)S(1)} all-to-all(bf16[2,4,128,256]{2,3,0,1:T(8,128)(2,1)S(1)} %copy.36), channel_id=1, replica_groups=mesh['sp'=8,'tp'=4] {'tp'}, dimensions={1} | all-to-all | bytes 1048576 | tf_op jit(solution)/shard_map/all_to_all | solution.py:309
  225.7 2.4 collective-permute-start.1
  228.1 8.1 %collective-permute-done.1 = bf16[128,1024]{0,1:T(8,128)(2,1)S(1)} collective-permute-done((bf16[128,1024]{0,1:T(8,128)(2,1)S(1)}, bf16[128,1024]{0,1:T(8,128)(2,1)S(1)}, u32[]{:S(2)}, u32[]{:S(2)}) %collective-permute-start.1) | collective-permute-done | bytes 262176 | tf_op jit(solution)/shard_map/ppermute | solution.py:316
  236.2 5.9 %multiply_reduce_fusion = (f32[256]{0:T(256)S(1)}, f32[256,4096]{1,0:T(8,128)S(1)}) fusion(bf16[1024,4096]{1,0:T(8,128)(2,1)} %param.20, bf16[128,1024]{0,1:T(8,128)(2,1)S(1)} %collective-permute-done.1, bf16[128,1024]{0,1:T(8,128)(2,1)S(1)} %bitcast.37), kind=kOutput, calls=%fused_computation.6 | convolution fusion | flops 2150629120 | bytes 13108224 | tf_op jit(solution)/shard_map/dot_general | solution.py:318
  242.1 1.9 multiply_convert_fusion
  (41 shorter events, 1.1 us)
Async XLA Ops:
  6.5 23.5 %copy-start = (bf16[4096,32]{0,1:T(8,128)(2,1)S(1)}, bf16[4096,32]{0,1:T(8,128)(2,1)}, u32[]{:S(2)}) copy-start(bf16[4096,32]{0,1:T(8,128)(2,1)} %param.15) | copy-start | bytes 786436
  6.5 42.0 %all-gather.3.cloned.1.call-start = ((), (), s32[]{:S(2)}) async-start(), calls=%async_computation.1 | async-start | bytes 1966080 | tf_op jit(solution)/shard_map/all_gather | solution.py:282
  8.7 5.6 %copy-start.7 = (f32[768]{0:T(1024)S(1)}, f32[768]{0:T(1024)}, u32[]{:S(2)}) copy-start(f32[768]{0:T(1024)} %param.16) | copy-start | bytes 9220
  8.7 17.7 %copy-start.4 = (bf16[256,4096]{1,0:T(8,128)(2,1)S(1)}, bf16[256,4096]{1,0:T(8,128)(2,1)}, u32[]{:S(2)}) copy-start(bf16[256,4096]{1,0:T(8,128)(2,1)} %param.11) | copy-start | bytes 6291460
  8.7 17.7 %copy-start.9 = (f32[4096]{0:T(1024)S(1)}, f32[4096]{0:T(1024)}, u32[]{:S(2)}) copy-start(f32[4096]{0:T(1024)} %param.12) | copy-start | bytes 49156
  14.4 11.1 %collective-permute-start = (bf16[128,768]{1,0:T(8,128)(2,1)S(1)}, bf16[128,768]{1,0:T(8,128)(2,1)S(1)}, u32[]{:S(2)}, u32[]{:S(2)}) collective-permute-start(bf16[128,768]{1,0:T(8,128)(2,1)S(1)} %get-tuple-element.8), channel_id=1, source_target_pairs={{0,28},{4,24},{8,20},{12,16},{16,12},{20,8},{24,4},{28,0},{1,29},{... | collective-permute-start | bytes 589832 | tf_op jit(solution)/shard_map/ppermute | solution.py:280
  26.3 111.3 %all-gather.5.cloned.1.call-start = ((), (), s32[]{:S(2)}) async-start(), calls=%async_computation.2 | async-start | bytes 10813440 | tf_op jit(solution)/shard_map/all_gather | solution.py:274
  29.9 1.4 copy-start.8
  30.0 2.5 copy-start.5
  30.0 2.8 %copy-start.1 = (bf16[512,512]{1,0:T(8,128)(2,1)S(1)}, bf16[512,512]{1,0:T(8,128)(2,1)}, u32[]{:S(2)}) copy-start(bf16[512,512]{1,0:T(8,128)(2,1)} %kv_up_ref.1) | copy-start | bytes 1572868
  137.6 0.9 copy-start.2
  138.6 0.8 copy-start.3
  225.7 10.5 %collective-permute-start.1 = (bf16[128,1024]{0,1:T(8,128)(2,1)S(1)}, bf16[128,1024]{0,1:T(8,128)(2,1)S(1)}, u32[]{:S(2)}, u32[]{:S(2)}) collective-permute-start(bf16[128,1024]{0,1:T(8,128)(2,1)S(1)} %bitcast.38), channel_id=1, source_target_pairs={{0,28},{4,24},{8,20},{12,16},{16,12},{20,8},{24,4},{28,0},{1,29},{... | collective-permute-start | bytes 786440 | tf_op jit(solution)/shard_map/ppermute | solution.py:316
  236.2 5.9 %copy-start.6 = (f32[4096]{0:T(1024)S(1)}, f32[4096]{0:T(1024)}, u32[]{:S(2)}) copy-start(f32[4096]{0:T(1024)} %param.21) | copy-start | bytes 49156
Sparse Core Ops, SparseCore 0:
  26.4 22.1 all-gather.2
  51.4 86.1 all-gather.4

commit v2 on v1

--- a/solution.py
+++ b/solution.py
@@ -230,6 +230,218 @@
     )(place, q_lat, q_up, cosine, sine, position, latents, kv_up, v_up)
 
 
+def plane_place(x, y, x_count, y_count):
+    down = y_count - 1 - y
+    across = jnp.where(lax.rem(down, 2) == 0, x - 1, x_count - 1 - x)
+    return jnp.where(x == 0, y, y_count + down * (x_count - 1) + across)
+
+
+def plane_chip(place, x_count, y_count):
+    rest = jnp.maximum(place - y_count, 0)
+    down = lax.div(rest, x_count - 1)
+    step = lax.rem(rest, x_count - 1)
+    across = jnp.where(lax.rem(down, 2) == 0, 1 + step, x_count - 1 - step)
+    first = place < y_count
+    return jnp.where(first, 0, across), jnp.where(first, place, y_count - 1 - down)
+
+
+def ring_offsets(count):
+    order = [0]
+    for distance in range(1, count // 2 + 1):
+        order.append(distance)
+        if distance < count - distance:
+            order.append(-distance)
+    return order
+
+
+def gather_kernel(
+    sp_count, tp_count, lat_ref, q_ref, all_ref, q_all_ref, send_sem, recv_sem, q_send, q_recv, own_sem
+):
+    rows = lat_ref.shape[0]
+    half = rows // 2
+    y_count = tp_count // 2
+    x_count = y_count
+    z_count = sp_count // x_count
+    plane_count = x_count * y_count
+    sp = lax.axis_index("sp")
+    tp = lax.axis_index("tp")
+    z, x = lax.div(sp, x_count), lax.rem(sp, x_count)
+    y, core = lax.div(tp, 2), lax.rem(tp, 2)
+    plane = plane_place(x, y, x_count, y_count)
+    mate = sp_count - 1 - sp
+
+    def device(z_at, plane_at, core_at):
+        x_at, y_at = plane_chip(plane_at, x_count, y_count)
+        return z_at * x_count + x_at, y_at * 2 + core_at
+
+    def wrap(value, count):
+        return lax.rem(value + count, count)
+
+    z_up, z_down = wrap(z + 1, z_count), wrap(z - 1, z_count)
+    p_up, p_down = wrap(plane + 1, plane_count), wrap(plane - 1, plane_count)
+    neighbours = [
+        device(z_up, plane, core),
+        device(z_down, plane, core),
+        device(z, p_up, core),
+        device(z, p_down, core),
+    ]
+    others = [wrap(tp + step, tp_count) for step in range(1, tp_count)]
+    greeted = neighbours + [(sp, other) for other in others]
+    greeted += [(mate, wrap(tp + step, tp_count)) for step in range(tp_count)]
+    barrier = pltpu.get_barrier_semaphore()
+    for target in greeted:
+        pl.semaphore_signal(
+            barrier, inc=1, device_id=target, device_id_type=pl.DeviceIdType.MESH
+        )
+    pl.semaphore_wait(barrier, len(greeted))
+
+    own_slot = sp * tp_count + tp
+    own_copies = [
+        pltpu.make_async_copy(lat_ref, all_ref.at[own_slot], own_sem.at[0]),
+        pltpu.make_async_copy(q_ref.at[pl.ds(0, half)], q_all_ref.at[0, tp], own_sem.at[1]),
+    ]
+    for copy in own_copies:
+        copy.start()
+
+    def q_copy(side, target, index):
+        return pltpu.make_async_remote_copy(
+            src_ref=q_ref.at[pl.ds(side * half, half)],
+            dst_ref=q_all_ref.at[side, tp],
+            send_sem=q_send.at[index],
+            recv_sem=q_recv.at[side, tp],
+            device_id=target,
+            device_id_type=pl.DeviceIdType.MESH,
+        )
+
+    q_copies = [q_copy(0, (sp, other), index) for index, other in enumerate(others)]
+    q_copies += [
+        q_copy(1, (mate, wrap(tp + step, tp_count)), tp_count - 1 + step)
+        for step in range(tp_count)
+    ]
+
+    def spread(core_at, count_1, count_2, at_1, at_2, place):
+        sent = []
+
+        def part(slot, piece):
+            return all_ref.at[slot, pl.ds(piece * half, half)]
+
+        def slot_of(one, two, core_of):
+            sp_of, tp_of = device(*place(one, two), core_of)
+            return sp_of * tp_count + tp_of
+
+        def push(slot, piece, target, mine):
+            source = lat_ref.at[pl.ds(piece * half, half)] if mine else part(slot, piece)
+            copy = pltpu.make_async_remote_copy(
+                src_ref=source,
+                dst_ref=part(slot, piece),
+                send_sem=send_sem.at[len(sent)],
+                recv_sem=recv_sem.at[slot, piece],
+                device_id=target,
+                device_id_type=pl.DeviceIdType.MESH,
+            )
+            copy.start()
+            sent.append(copy)
+
+        def arrive(slot, piece):
+            pltpu.make_async_remote_copy(
+                src_ref=part(slot, piece),
+                dst_ref=part(slot, piece),
+                send_sem=send_sem.at[0],
+                recv_sem=recv_sem.at[slot, piece],
+                device_id=neighbours[0],
+                device_id_type=pl.DeviceIdType.MESH,
+            ).wait_recv()
+
+        def onward(slot, offset, piece, count, up, down, mine):
+            far = count // 2
+            if offset <= 0 and offset != far:
+                distance = 1 - offset
+                if distance < far or (distance == far and piece == 1):
+                    push(slot, piece, down, mine)
+            if offset >= 0 and offset != far:
+                distance = 1 + offset
+                if distance < far or (distance == far and piece == 0):
+                    push(slot, piece, up, mine)
+
+        up_1 = device(*place(wrap(at_1 + 1, count_1), at_2), core_at)
+        down_1 = device(*place(wrap(at_1 - 1, count_1), at_2), core_at)
+        up_2 = device(*place(at_1, wrap(at_2 + 1, count_2)), core_at)
+        down_2 = device(*place(at_1, wrap(at_2 - 1, count_2)), core_at)
+        partner = (sp, y * 2 + 1 - core_at)
+        items = [(one, two) for one in ring_offsets(count_1) for two in ring_offsets(count_2)]
+        items.sort(key=lambda item: (abs(item[0]) + abs(item[1]), abs(item[1])))
+        for one, two in items:
+            slot = slot_of(wrap(at_1 - one, count_1), wrap(at_2 - two, count_2), core_at)
+            mine = one == 0 and two == 0
+            for piece in range(2):
+                if not mine:
+                    arrive(slot, piece)
+                if two == 0:
+                    onward(slot, one, piece, count_1, up_1, down_1, mine)
+                onward(slot, two, piece, count_2, up_2, down_2, mine)
+                push(slot, piece, partner, mine)
+            if mine:
+                for copy in q_copies:
+                    copy.start()
+        for one, two in items:
+            slot = slot_of(wrap(at_1 - one, count_1), wrap(at_2 - two, count_2), 1 - core_at)
+            for piece in range(2):
+                arrive(slot, piece)
+        for copy in sent:
+            copy.wait_send()
+
+    @pl.when(core == 0)
+    def _():
+        spread(0, plane_count, z_count, plane, z, lambda one, two: (two, one))
+
+    @pl.when(core == 1)
+    def _():
+        spread(1, z_count, plane_count, z, plane, lambda one, two: (one, two))
+
+    for index, copy in enumerate(q_copies):
+        copy.wait_send()
+    for side, source in [(0, other) for other in others] + [(1, at) for at in range(tp_count)]:
+        pltpu.make_async_remote_copy(
+            src_ref=q_all_ref.at[side, source],
+            dst_ref=q_all_ref.at[side, source],
+            send_sem=q_send.at[0],
+            recv_sem=q_recv.at[side, source],
+            device_id=neighbours[0],
+            device_id_type=pl.DeviceIdType.MESH,
+        ).wait_recv()
+    for copy in own_copies:
+        copy.wait()
+
+
+def gather(latents, q_lat):
+    sp_count = lax.axis_size("sp")
+    tp_count = lax.axis_size("tp")
+    rows, width = latents.shape
+    count = sp_count * tp_count
+    space = pl.BlockSpec(memory_space=pltpu.VMEM)
+    everywhere, q_all = pl.pallas_call(
+        functools.partial(gather_kernel, sp_count, tp_count),
+        out_shape=(
+            jax.ShapeDtypeStruct((count, rows, width), latents.dtype),
+            jax.ShapeDtypeStruct((2, tp_count, rows // 2, q_lat.shape[1]), q_lat.dtype),
+        ),
+        in_specs=[space, space],
+        out_specs=(pl.BlockSpec(memory_space=pl.ANY), pl.BlockSpec(memory_space=pl.ANY)),
+        scratch_shapes=[
+            pltpu.SemaphoreType.DMA((4 * count,)),
+            pltpu.SemaphoreType.DMA((count, 2)),
+            pltpu.SemaphoreType.DMA((2 * tp_count,)),
+            pltpu.SemaphoreType.DMA((2, tp_count)),
+            pltpu.SemaphoreType.DMA((2,)),
+        ],
+        compiler_params=pltpu.CompilerParams(collective_id=0, has_side_effects=True),
+        cost_estimate=pl.CostEstimate(
+            flops=0, bytes_accessed=count * rows * width * 8, transcendentals=0
+        ),
+    )(latents, q_lat)
+    return everywhere.reshape(count * rows, width), q_all.reshape(tp_count * rows, -1)
+
+
 def local(
     tokens,
     norm_gain,
@@ -271,18 +483,11 @@
         ],
         axis=1,
     )
-    latents = lax.all_gather(packed, ("sp", "tp"), axis=0, tiled=True)
-
     q_lat = scaled_norm(jnp.dot(normed, q_down, preferred_element_type=jnp.float32), q_gain).astype(
         jnp.bfloat16
     )
     swap = [(place, sp_count - 1 - place) for place in range(sp_count)]
-    other = lax.ppermute(q_lat[half:], "sp", swap)
-    q_pair = jnp.concatenate([q_lat[:half], other], axis=0)
-    q_group = lax.all_gather(q_pair, "tp", axis=0, tiled=True)
-    q_group = (
-        q_group.reshape(tp_count, 2, half, -1).transpose(1, 0, 2, 3).reshape(group_rows, -1)
-    )
+    latents, q_group = gather(packed, q_lat)
     mate = sp_count - 1 - sp_place
     base = jnp.stack([sp_place * group_rows, mate * group_rows + half])
     position = (

time: 251 us -> 220 us (0.88)
  waiting for transfers between devices: 114 us -> 9.62 us
  Pallas kernels: 74.6 us -> 172 us
  between operations: 13.6 us -> 0.23 us
  starting transfers between devices: 8.54 us -> 0.93 us
  local copies, waits for them, and re-layouts: 5.84 us -> 3.23 us
    all_gather x2 -> x0, waiting for transfers between devices: 101 us -> none  [the longest x1 87.5 us: local(): latents = lax.all_gather(packed, ('sp', 'tp'), axis=0, tiled=True)]
    pallas_call x0 -> x1, Pallas kernels: none -> 97.2 us  [gather(): pl.pallas_call(functools.partial(gather_kernel, sp_count, tp_count), out_...]
    ppermute x1 -> x0, starting transfers between devices: 6.06 us -> none  [local(): other = lax.ppermute(q_lat[half:], 'sp', swap)]
    ppermute x1 -> x0, waiting for transfers between devices: 5 us -> none  [local(): other = lax.ppermute(q_lat[half:], 'sp', swap)]
    dot_general x1, matrix products: 5.51 us -> 2.84 us  [local(): jnp.dot(normed, q_down, preferred_element_type=jnp.float32)]
  transfers between devices with their start and end apart: 4 -> 1, of which waited for: 4 -> 1; matrix products, arithmetic and copies ran while one was open for 4% -> 0% of each run, Pallas kernels for 0% -> 0%
where the time goes in v2:
time: 220 us
  Pallas kernels  172 us (78%)
  matrix products  14.1 us (6%)
  blocking collectives  11.2 us (5%)
  waiting for transfers between devices  9.62 us (4%)
  other arithmetic  8.39 us (4%)
  local copies, waits for them, and re-layouts  3.23 us (1%)
    pallas_call x1, Pallas kernels, gather(): pl.pallas_call(functools.partial(gather_kernel, sp_count, tp_count), out_...  97.2 us
    pallas_call x1, Pallas kernels, attend(): pl.pallas_call(functools.partial(attend_kernel, rows, heads, group_rows,...  74.7 us
    all_to_all x1, blocking collectives, local(): lax.all_to_all(attended.reshape(2, tp_count, half, heads * VDIM), 'tp', s...  11.2 us
    ppermute x1, waiting for transfers between devices, local(): returned = lax.ppermute(own_heads[1, 0], 'sp', swap)  9.62 us
    dot_general x1, matrix products, local(): jnp.dot(own_rows, out_weight, preferred_element_type=jnp.float32)  5.89 us
  transfers between devices with their start and end apart: 1, of which 1 were waited for; matrix products, arithmetic and copies ran while one was open for 0% of the time, Pallas kernels for 0%

profile of v2, /device:TPU:0, one launch (start us, length us, event | category | flops | bytes accessed | tf_op | source)
XLA Modules:
  0.0 219.6 jit_solution(8836481840594114332)
XLA Ops:
  0.1 2.2 %fusion = f32[256]{0:T(256)S(1)} fusion(bf16[256,4096]{1,0:T(8,128)(2,1)} %param.11), kind=kLoop, calls=%fused_computation.2 | loop fusion | flops 3145472 | bytes 2098176 | tf_op jit(solution)/shard_map/reduce_sum | solution.py:27
  2.3 3.3 %fusion.19 = f32[256,32]{1,0:T(8,128)} fusion(bf16[4096,32]{0,1:T(8,128)(2,1)S(1)} %copy-done, bf16[256,4096]{1,0:T(8,128)(2,1)} %param.11, f32[4096]{0:T(1024)} %param.12, f32[256]{0:T(256)S(1)} %add_rsqrt_fusion.3), kind=kOutput, calls=%fused_computation.42 | convolution fusion | flops 71303168 | bytes 2409472 | tf_op jit(solution)/shard_map/dot_general | solution.py:475
  5.6 2.1 multiply_reduce_fusion.2
  7.8 2.8 %multiply_reduce_fusion.1 = (f32[256]{0:T(256)S(1)}, f32[256,768]{1,0:T(8,128)}) fusion(bf16[4096,768]{1,0:T(8,128)(2,1)S(1)} %bitcast.39, bf16[256,4096]{1,0:T(8,128)(2,1)S(1)} %copy-done.3, f32[4096]{0:T(1024)S(1)} %copy-done.10, f32[256]{0:T(256)S(1)} %add_rsqrt_fusion.3), kind=kOutput, calls=%fused_computation.8 | convolution fusion | flops 1615200000 | bytes 9193472 | tf_op jit(solution)/shard_map/dot_general | solution.py:486
  10.6 0.1 pad_add_fusion.1
  10.7 0.1 broadcast_add_fusion
  10.8 0.1 iota_add_fusion
  10.9 0.2 copy.35
  11.1 0.3 copy.30
  11.4 0.3 multiply_sine_fusion.1
  11.7 1.6 fusion.14
  13.3 1.2 multiply_convert_fusion.2
  14.4 0.9 multiply_convert_fusion.1.q_ref
  15.4 0.9 concatenate.9.lat_ref
  16.3 97.2 %shard_map.109 = (bf16[32,256,640]{2,1,0:T(8,128)(2,1)}, bf16[2,4,128,768]{3,2,1,0:T(8,128)(2,1)}) custom-call(bf16[256,640]{1,0:T(8,128)(2,1)} %concatenate.9.lat_ref, bf16[256,768]{1,0:T(8,128)(2,1)} %multiply_convert_fusion.1.q_ref), custom_call_target="tpu_custom_call" | custom-call | bytes 41943040 | tf_op jit(solution)/shard_map/pallas_call | solution.py:422
  113.4 0.1 pad_add_fusion.place_ref
  113.5 1.4 copy-done.2
  114.9 74.7 %shard_map.110 = bf16[1024,256]{1,0:T(8,128)(2,1)S(1)} custom-call(s32[2]{0:T(128)S(1)} %pad_add_fusion.place_ref, bf16[1024,768]{1,0:T(8,128)(2,1)S(1)} %bitcast.31, bf16[4,96,768]{2,1,0:T(8,128)(2,1)S(1)} %bitcast.27, f32[16,1024]{1,0:T(8,128)S(1)} %get-tuple-element.14.cos_ref, f32[16,1024]{1,0:T(8,128)S(1)} %get-tuple-element.13.sin_ref, ...), custom_call_target="tpu_custom_call" | custom-call | flops 10737418240 | bytes 10485760 | tf_op jit(solution)/shard_map/pallas_call | solution.py:193
  189.6 0.3 copy.32
  189.9 11.2 %all_to_all.15 = bf16[2,4,128,256]{2,3,0,1:T(8,128)(2,1)S(1)} all-to-all(bf16[2,4,128,256]{2,3,0,1:T(8,128)(2,1)S(1)} %copy.32), channel_id=1, replica_groups=mesh['sp'=8,'tp'=4] {'tp'}, dimensions={1} | all-to-all | bytes 1048576 | tf_op jit(solution)/shard_map/all_to_all | solution.py:514
  201.2 0.9 collective-permute-start
  202.1 9.6 %collective-permute-done = bf16[128,1024]{0,1:T(8,128)(2,1)S(1)} collective-permute-done((bf16[128,1024]{0,1:T(8,128)(2,1)S(1)}, bf16[128,1024]{0,1:T(8,128)(2,1)S(1)}, u32[]{:S(2)}, u32[]{:S(2)}) %collective-permute-start) | collective-permute-done | bytes 262176 | tf_op jit(solution)/shard_map/ppermute | solution.py:521
  211.7 5.9 %multiply_reduce_fusion = (f32[256]{0:T(256)S(1)}, f32[256,4096]{1,0:T(8,128)S(1)}) fusion(bf16[1024,4096]{1,0:T(8,128)(2,1)} %param.20, bf16[128,1024]{0,1:T(8,128)(2,1)S(1)} %collective-permute-done, bf16[128,1024]{0,1:T(8,128)(2,1)S(1)} %bitcast.34), kind=kOutput, calls=%fused_computation.6 | convolution fusion | flops 2150629120 | bytes 13108224 | tf_op jit(solution)/shard_map/dot_general | solution.py:523
  217.7 1.9 multiply_convert_fusion
  (38 shorter events, 0.2 us)
Async XLA Ops:
  0.0 2.3 %copy-start = (bf16[4096,32]{0,1:T(8,128)(2,1)S(1)}, bf16[4096,32]{0,1:T(8,128)(2,1)}, u32[]{:S(2)}) copy-start(bf16[4096,32]{0,1:T(8,128)(2,1)} %param.15) | copy-start | bytes 786436
  0.0 5.6 %copy-start.3 = (bf16[256,4096]{1,0:T(8,128)(2,1)S(1)}, bf16[256,4096]{1,0:T(8,128)(2,1)}, u32[]{:S(2)}) copy-start(bf16[256,4096]{1,0:T(8,128)(2,1)} %param.11) | copy-start | bytes 6291460
  0.0 5.6 %copy-start.10 = (f32[4096]{0:T(1024)S(1)}, f32[4096]{0:T(1024)}, u32[]{:S(2)}) copy-start(f32[4096]{0:T(1024)} %param.12) | copy-start | bytes 49156
  0.0 5.6 %copy-start.9 = (bf16[4096,512]{1,0:T(8,128)(2,1)S(1)}, bf16[4096,512]{1,0:T(8,128)(2,1)}, u32[]{:S(2)}) copy-start(bf16[4096,512]{1,0:T(8,128)(2,1)} %param.14) | copy-start | bytes 12582916
  2.3 5.4 %slice-start = ((s8[6291456]{0:T(1024)(128)(4,1)}), s8[4194304]{0:T(1024)(128)(4,1)S(1)}, s32[]{:S(2)}) async-start(s8[6291456]{0:T(1024)(128)(4,1)} %bitcast.38), calls=%async_computation.1 | async-start | bytes 8388608
  5.6 2.1 slice-start.1
  7.7 3.1 %copy-start.1 = (bf16[512,512]{1,0:T(8,128)(2,1)S(1)}, bf16[512,512]{1,0:T(8,128)(2,1)}, u32[]{:S(2)}) copy-start(bf16[512,512]{1,0:T(8,128)(2,1)} %kv_up_ref.1) | copy-start | bytes 1572868
  7.7 3.4 %copy-start.5 = (bf16[768,384]{1,0:T(8,128)(2,1)S(1)}, bf16[768,384]{1,0:T(8,128)(2,1)}, u32[]{:S(2)}) copy-start(bf16[768,384]{1,0:T(8,128)(2,1)} %param.18) | copy-start | bytes 1769476
  7.7 5.5 %copy-start.8 = (f32[512]{0:T(512)S(1)}, f32[512]{0:T(512)}, u32[]{:S(2)}) copy-start(f32[512]{0:T(512)} %param.17) | copy-start | bytes 6148
  7.8 6.7 %copy-start.7 = (f32[768]{0:T(1024)S(1)}, f32[768]{0:T(1024)}, u32[]{:S(2)}) copy-start(f32[768]{0:T(1024)} %param.16) | copy-start | bytes 9220
  10.6 3.8 %copy-start.4 = (f32[256,768]{1,0:T(8,128)S(1)}, f32[256,768]{1,0:T(8,128)}, u32[]{:S(2)}) copy-start(f32[256,768]{1,0:T(8,128)} %get-tuple-element.20) | copy-start | bytes 2359300
  113.5 1.4 copy-start.2
  201.2 10.5 %collective-permute-start = (bf16[128,1024]{0,1:T(8,128)(2,1)S(1)}, bf16[128,1024]{0,1:T(8,128)(2,1)S(1)}, u32[]{:S(2)}, u32[]{:S(2)}) collective-permute-start(bf16[128,1024]{0,1:T(8,128)(2,1)S(1)} %bitcast.35), channel_id=1, source_target_pairs={{0,28},{4,24},{8,20},{12,16},{16,12},{20,8},{24,4},{28,0},{1,29},{... | collective-permute-start | bytes 786440 | tf_op jit(solution)/shard_map/ppermute | solution.py:521
  211.7 5.9 %copy-start.6 = (f32[4096]{0:T(1024)S(1)}, f32[4096]{0:T(1024)}, u32[]{:S(2)}) copy-start(f32[4096]{0:T(1024)} %param.21) | copy-start | bytes 49156

commit v3 on v2

--- a/solution.py
+++ b/solution.py
@@ -16,7 +16,7 @@
 THETA = 500000.0
 LOG2E = 1.4426950408889634
 FLOOR = -1e30
-Q_TILE = 256
+Q_TILE = 512
 K_TILE = 512
 V_ROWS = VDIM + 16
 
@@ -54,6 +54,7 @@
     sin_ref,
     position_ref,
     lat_ref,
+    turned_ref,
     kv_up_ref,
     v_up_ref,
     out_ref,
@@ -97,8 +98,8 @@
 
     @pl.when(chunk <= jnp.maximum(own, mate))
     def _():
-        lat = lat_ref[:, :rank]
-        turned = lat_ref[:, rank:]
+        lat = lat_ref[...].reshape(group_rows, rank)
+        turned = turned_ref[...]
         lane = lax.broadcasted_iota(jnp.int32, (group_rows, HEAD_KV), 1)
         for head in range(heads):
             raw = jnp.dot(
@@ -126,7 +127,12 @@
                     + lax.broadcasted_iota(jnp.int32, (K_TILE, Q_TILE), 0)
                 )
                 visible = key_index <= position_ref[:, columns]
-            for head in range(heads):
+            every = range(heads)
+            old = [top_ref[head, :, columns] for head in every]
+            before = [sum_ref[head, :, columns] for head in every]
+            new = []
+            after = []
+            for head in every:
                 scores = jnp.dot(
                     key_ref[head, keys, :],
                     query_ref[head, :, columns],
@@ -134,18 +140,18 @@
                 )
                 if masked:
                     scores = jnp.where(visible, scores, FLOOR)
-                old = top_ref[head, :, columns]
-                new = jnp.maximum(old, jnp.max(scores, axis=0, keepdims=True))
-                weights = jnp.exp2((scores - new) * scale)
+                top = jnp.maximum(old[head], jnp.max(scores, axis=0, keepdims=True))
+                weights = jnp.exp2((scores - top) * scale)
                 product = jnp.dot(
                     value_ref[head, :, keys],
                     weights.astype(jnp.bfloat16),
                     preferred_element_type=jnp.float32,
                 )
-                sum_ref[head, :, columns] = (
-                    sum_ref[head, :, columns] * jnp.exp2((old - new) * scale) + product
-                )
-                top_ref[head, :, columns] = new
+                new.append(top)
+                after.append(before[head] * jnp.exp2((old[head] - top) * scale) + product)
+            for head in every:
+                sum_ref[head, :, columns] = after[head]
+                top_ref[head, :, columns] = new[head]
 
         @pl.loop(0, key_steps * query_steps)
         def _(index):
@@ -180,16 +186,17 @@
             out_ref[columns, :] = jnp.concatenate(parts, axis=0).T.astype(jnp.bfloat16)
 
 
-def attend(place, q_lat, q_up, cosine, sine, position, latents, kv_up, v_up, rows):
+def attend(place, q_lat, q_up, cosine, sine, position, latents, turned, kv_up, v_up, rows):
     group_rows, q_rank = q_lat.shape
     heads = q_up.shape[0]
     rank = kv_up.shape[0]
-    chunks = latents.shape[0] // group_rows
+    chunks = turned.shape[0] // group_rows
+    tp_count = group_rows // rows
 
     def whole(*shape):
         return pl.BlockSpec(shape, lambda chunk, place_ref: (0,) * len(shape))
 
-    pairs = latents.shape[0] * group_rows * heads // 2
+    pairs = turned.shape[0] * group_rows * heads // 2
     return pl.pallas_call(
         functools.partial(attend_kernel, rows, heads, group_rows, rank),
         out_shape=jax.ShapeDtypeStruct((group_rows, heads * VDIM), jnp.bfloat16),
@@ -203,12 +210,14 @@
                 whole(ROPE // 2, group_rows),
                 whole(1, group_rows),
                 pl.BlockSpec(
-                    (group_rows, latents.shape[1]),
+                    (tp_count, rows, rank),
                     lambda chunk, place_ref: (
                         jnp.minimum(chunk, jnp.maximum(place_ref[0], place_ref[1])),
                         0,
+                        0,
                     ),
                 ),
+                pl.BlockSpec((group_rows, HEAD_KV), lambda chunk, place_ref: (chunk, 0)),
                 whole(*kv_up.shape),
                 whole(*v_up.shape),
             ],
@@ -227,7 +236,7 @@
         cost_estimate=pl.CostEstimate(
             flops=pairs * 640, bytes_accessed=latents.size * 2, transcendentals=pairs
         ),
-    )(place, q_lat, q_up, cosine, sine, position, latents, kv_up, v_up)
+    )(place, q_lat, q_up, cosine, sine, position, latents, turned, kv_up, v_up)
 
 
 def plane_place(x, y, x_count, y_count):
@@ -257,8 +266,9 @@
 def gather_kernel(
     sp_count, tp_count, lat_ref, q_ref, all_ref, q_all_ref, send_sem, recv_sem, q_send, q_recv, own_sem
 ):
-    rows = lat_ref.shape[0]
-    half = rows // 2
+    half = q_ref.shape[0] // 2
+    extra = lat_ref.shape[0] - 2 * half
+    starts, sizes = (0, half + extra), (half + extra, half)
     y_count = tp_count // 2
     x_count = y_count
     z_count = sp_count // x_count
@@ -287,7 +297,7 @@
     ]
     others = [wrap(tp + step, tp_count) for step in range(1, tp_count)]
     greeted = neighbours + [(sp, other) for other in others]
-    greeted += [(mate, wrap(tp + step, tp_count)) for step in range(tp_count)]
+    greeted += [(mate, tp)]
     barrier = pltpu.get_barrier_semaphore()
     for target in greeted:
         pl.semaphore_signal(
@@ -303,34 +313,103 @@
     for copy in own_copies:
         copy.start()
 
-    def q_copy(side, target, index):
+    sames = [wrap(tp + 2 * step, tp_count) for step in range(1, y_count)]
+    partner_tp = y * 2 + 1 - core
+
+    def q_copy(side, source, target, index, mine):
+        landed = q_all_ref.at[side, source]
         return pltpu.make_async_remote_copy(
-            src_ref=q_ref.at[pl.ds(side * half, half)],
-            dst_ref=q_all_ref.at[side, tp],
+            src_ref=q_ref.at[pl.ds(side * half, half)] if mine else landed,
+            dst_ref=landed,
             send_sem=q_send.at[index],
-            recv_sem=q_recv.at[side, tp],
+            recv_sem=q_recv.at[side, source],
             device_id=target,
             device_id_type=pl.DeviceIdType.MESH,
         )
 
-    q_copies = [q_copy(0, (sp, other), index) for index, other in enumerate(others)]
-    q_copies += [
-        q_copy(1, (mate, wrap(tp + step, tp_count)), tp_count - 1 + step)
-        for step in range(tp_count)
-    ]
-
-    def spread(core_at, count_1, count_2, at_1, at_2, place):
+    q_copies = []
+
+    def q_push(side, source, target, mine):
+        copy = q_copy(side, source, target, len(q_copies), mine)
+        copy.start()
+        q_copies.append(copy)
+
+    q_push(1, tp, (mate, tp), True)
+    for same in sames:
+        q_push(0, tp, (sp, same), True)
+    q_push(0, tp, (sp, partner_tp), True)
+    q_first = tuple(q_copies)
+
+    def finish_q():
+        del q_copies[len(q_first) :]
+        q_copy(1, tp, (mate, tp), 0, False).wait_recv()
+        for same in sames:
+            q_push(1, tp, (sp, same), False)
+        q_push(1, tp, (sp, partner_tp), False)
+        for side in range(2):
+            for same in sames:
+                q_copy(side, same, (mate, tp), 0, False).wait_recv()
+                q_push(side, same, (sp, partner_tp), False)
+        for side in range(2):
+            for at in range(y_count):
+                q_copy(side, at * 2 + 1 - core, (mate, tp), 0, False).wait_recv()
+        for copy in q_copies:
+            copy.wait_send()
+
+    def when(condition, action):
+        if condition is None:
+            action()
+        else:
+            pl.when(condition)(action)
+
+    def both(left, right):
+        if left is None or right is None:
+            return right if left is None else left
+        return left & right
+
+    def ring_sends(offset, piece, count, at, line):
+        ways = []
+        if line:
+            if offset >= 0:
+                ways.append((0, at + 1 < count))
+            if offset <= 0:
+                ways.append((1, at > 0))
+            return ways
+        far = count // 2
+        if offset <= 0 and offset != far:
+            distance = 1 - offset
+            if distance < far or (distance == far and piece == 1):
+                ways.append((1, None))
+        if offset >= 0 and offset != far:
+            distance = 1 + offset
+            if distance < far or (distance == far and piece == 0):
+                ways.append((0, None))
+        return ways
+
+    def offsets_of(count, line):
+        if not line:
+            return ring_offsets(count)
+        return [0] + [sign * step for step in range(1, count) for sign in (1, -1)]
+
+    def exists(offset, count, at, line):
+        if not line or offset == 0:
+            return None
+        return at >= offset if offset > 0 else at - offset < count
+
+    def spread(core_at, count_1, count_2, at_1, at_2, line_1, line_2, place):
         sent = []
 
         def part(slot, piece):
-            return all_ref.at[slot, pl.ds(piece * half, half)]
+            return all_ref.at[slot, pl.ds(starts[piece], sizes[piece])]
 
         def slot_of(one, two, core_of):
             sp_of, tp_of = device(*place(one, two), core_of)
             return sp_of * tp_count + tp_of
 
-        def push(slot, piece, target, mine):
-            source = lat_ref.at[pl.ds(piece * half, half)] if mine else part(slot, piece)
+        def push(slot, piece, target, mine, condition):
+            source = (
+                lat_ref.at[pl.ds(starts[piece], sizes[piece])] if mine else part(slot, piece)
+            )
             copy = pltpu.make_async_remote_copy(
                 src_ref=source,
                 dst_ref=part(slot, piece),
@@ -339,76 +418,64 @@
                 device_id=target,
                 device_id_type=pl.DeviceIdType.MESH,
             )
-            copy.start()
-            sent.append(copy)
-
-        def arrive(slot, piece):
-            pltpu.make_async_remote_copy(
+            when(condition, copy.start)
+            sent.append((copy, condition))
+
+        def arrive(slot, piece, condition):
+            copy = pltpu.make_async_remote_copy(
                 src_ref=part(slot, piece),
                 dst_ref=part(slot, piece),
                 send_sem=send_sem.at[0],
                 recv_sem=recv_sem.at[slot, piece],
                 device_id=neighbours[0],
                 device_id_type=pl.DeviceIdType.MESH,
-            ).wait_recv()
-
-        def onward(slot, offset, piece, count, up, down, mine):
-            far = count // 2
-            if offset <= 0 and offset != far:
-                distance = 1 - offset
-                if distance < far or (distance == far and piece == 1):
-                    push(slot, piece, down, mine)
-            if offset >= 0 and offset != far:
-                distance = 1 + offset
-                if distance < far or (distance == far and piece == 0):
-                    push(slot, piece, up, mine)
-
-        up_1 = device(*place(wrap(at_1 + 1, count_1), at_2), core_at)
-        down_1 = device(*place(wrap(at_1 - 1, count_1), at_2), core_at)
-        up_2 = device(*place(at_1, wrap(at_2 + 1, count_2)), core_at)
-        down_2 = device(*place(at_1, wrap(at_2 - 1, count_2)), core_at)
+            )
+            when(condition, copy.wait_recv)
+
+        ways_1 = [
+            device(*place(wrap(at_1 + step, count_1), at_2), core_at) for step in (1, -1)
+        ]
+        ways_2 = [
+            device(*place(at_1, wrap(at_2 + step, count_2)), core_at) for step in (1, -1)
+        ]
         partner = (sp, y * 2 + 1 - core_at)
-        items = [(one, two) for one in ring_offsets(count_1) for two in ring_offsets(count_2)]
+        items = [
+            (one, two)
+            for one in offsets_of(count_1, line_1)
+            for two in offsets_of(count_2, line_2)
+        ]
         items.sort(key=lambda item: (abs(item[0]) + abs(item[1]), abs(item[1])))
+        swapped = []
         for one, two in items:
             slot = slot_of(wrap(at_1 - one, count_1), wrap(at_2 - two, count_2), core_at)
             mine = one == 0 and two == 0
+            here = both(exists(one, count_1, at_1, line_1), exists(two, count_2, at_2, line_2))
             for piece in range(2):
                 if not mine:
-                    arrive(slot, piece)
+                    arrive(slot, piece, here)
                 if two == 0:
-                    onward(slot, one, piece, count_1, up_1, down_1, mine)
-                onward(slot, two, piece, count_2, up_2, down_2, mine)
-                push(slot, piece, partner, mine)
-            if mine:
-                for copy in q_copies:
-                    copy.start()
-        for one, two in items:
-            slot = slot_of(wrap(at_1 - one, count_1), wrap(at_2 - two, count_2), 1 - core_at)
-            for piece in range(2):
-                arrive(slot, piece)
-        for copy in sent:
-            copy.wait_send()
+                    for way, condition in ring_sends(one, piece, count_1, at_1, line_1):
+                        push(slot, piece, ways_1[way], mine, both(here, condition))
+                for way, condition in ring_sends(two, piece, count_2, at_2, line_2):
+                    push(slot, piece, ways_2[way], mine, both(here, condition))
+                push(slot, piece, partner, mine, here)
+        finish_q()
+        for z_from in range(z_count):
+            for plane_from in range(plane_count):
+                sp_of, tp_of = device(z_from, plane_from, 1 - core_at)
+                for piece in range(2):
+                    arrive(sp_of * tp_count + tp_of, piece, None)
+        for copy, condition in sent:
+            when(condition, copy.wait_send)
 
     @pl.when(core == 0)
     def _():
-        spread(0, plane_count, z_count, plane, z, lambda one, two: (two, one))
+        spread(0, plane_count, z_count, plane, z, False, True, lambda one, two: (two, one))
 
     @pl.when(core == 1)
     def _():
-        spread(1, z_count, plane_count, z, plane, lambda one, two: (one, two))
-
-    for index, copy in enumerate(q_copies):
-        copy.wait_send()
-    for side, source in [(0, other) for other in others] + [(1, at) for at in range(tp_count)]:
-        pltpu.make_async_remote_copy(
-            src_ref=q_all_ref.at[side, source],
-            dst_ref=q_all_ref.at[side, source],
-            send_sem=q_send.at[0],
-            recv_sem=q_recv.at[side, source],
-            device_id=neighbours[0],
-            device_id_type=pl.DeviceIdType.MESH,
-        ).wait_recv()
+        spread(1, z_count, plane_count, z, plane, True, False, lambda one, two: (one, two))
+
     for copy in own_copies:
         copy.wait()
 
@@ -423,14 +490,14 @@
         functools.partial(gather_kernel, sp_count, tp_count),
         out_shape=(
             jax.ShapeDtypeStruct((count, rows, width), latents.dtype),
-            jax.ShapeDtypeStruct((2, tp_count, rows // 2, q_lat.shape[1]), q_lat.dtype),
+            jax.ShapeDtypeStruct((2, tp_count, q_lat.shape[0] // 2, q_lat.shape[1]), q_lat.dtype),
         ),
         in_specs=[space, space],
         out_specs=(pl.BlockSpec(memory_space=pl.ANY), pl.BlockSpec(memory_space=pl.ANY)),
         scratch_shapes=[
-            pltpu.SemaphoreType.DMA((4 * count,)),
+            pltpu.SemaphoreType.DMA((5 * count,)),
             pltpu.SemaphoreType.DMA((count, 2)),
-            pltpu.SemaphoreType.DMA((2 * tp_count,)),
+            pltpu.SemaphoreType.DMA((3 * tp_count,)),
             pltpu.SemaphoreType.DMA((2, tp_count)),
             pltpu.SemaphoreType.DMA((2,)),
         ],
@@ -439,7 +506,79 @@
             flops=0, bytes_accessed=count * rows * width * 8, transcendentals=0
         ),
     )(latents, q_lat)
-    return everywhere.reshape(count * rows, width), q_all.reshape(tp_count * rows, -1)
+    return everywhere, q_all.reshape(tp_count * q_lat.shape[0], -1)
+
+
+def deliver_kernel(sp_count, tp_count, in_ref, out_ref, send_sem, recv_sem, own_sem):
+    half = out_ref.shape[0] // 2
+    width = in_ref.shape[1]
+    sp = lax.axis_index("sp")
+    tp = lax.axis_index("tp")
+    mate = sp_count - 1 - sp
+    targets = [(0, sp, lax.rem(tp + step, tp_count)) for step in range(1, tp_count)]
+    targets = [(1, mate, lax.rem(tp + step, tp_count)) for step in range(tp_count)] + targets
+    barrier = pltpu.get_barrier_semaphore()
+    for _, group, place in targets:
+        pl.semaphore_signal(
+            barrier, inc=1, device_id=(group, place), device_id_type=pl.DeviceIdType.MESH
+        )
+    pl.semaphore_wait(barrier, len(targets))
+    columns = pl.ds(pl.multiple_of(tp * width, width), width)
+
+    def source(side, place):
+        first = pl.multiple_of((side * tp_count + place) * half, half)
+        return in_ref.at[pl.ds(first, half)]
+
+    copies = []
+    for index, (side, group, place) in enumerate(targets):
+        copy = pltpu.make_async_remote_copy(
+            src_ref=source(side, place),
+            dst_ref=out_ref.at[pl.ds(side * half, half), columns],
+            send_sem=send_sem.at[index],
+            recv_sem=recv_sem.at[side, tp],
+            device_id=(group, place),
+            device_id_type=pl.DeviceIdType.MESH,
+        )
+        copy.start()
+        copies.append(copy)
+    own = pltpu.make_async_copy(source(0, tp), out_ref.at[pl.ds(0, half), columns], own_sem)
+    own.start()
+    for side, _, place in targets:
+        landed = out_ref.at[
+            pl.ds(side * half, half), pl.ds(pl.multiple_of(place * width, width), width)
+        ]
+        pltpu.make_async_remote_copy(
+            src_ref=landed,
+            dst_ref=landed,
+            send_sem=send_sem.at[0],
+            recv_sem=recv_sem.at[side, place],
+            device_id=(mate, tp),
+            device_id_type=pl.DeviceIdType.MESH,
+        ).wait_recv()
+    own.wait()
+    for copy in copies:
+        copy.wait_send()
+
+
+def deliver(attended):
+    sp_count = lax.axis_size("sp")
+    tp_count = lax.axis_size("tp")
+    group_rows, width = attended.shape
+    space = pl.BlockSpec(memory_space=pltpu.VMEM)
+    return pl.pallas_call(
+        functools.partial(deliver_kernel, sp_count, tp_count),
+        out_shape=jax.ShapeDtypeStruct(
+            (group_rows // tp_count, tp_count * width), attended.dtype
+        ),
+        in_specs=[space],
+        out_specs=space,
+        scratch_shapes=[
+            pltpu.SemaphoreType.DMA((2 * tp_count,)),
+            pltpu.SemaphoreType.DMA((2, tp_count)),
+            pltpu.SemaphoreType.DMA,
+        ],
+        compiler_params=pltpu.CompilerParams(collective_id=1, has_side_effects=True),
+    )(attended)
 
 
 def local(
@@ -474,20 +613,22 @@
     key_rot = rotate(
         jnp.dot(normed, rope_down, preferred_element_type=jnp.float32), own_position
     ).astype(jnp.bfloat16)
+    rot_rows = rows * ROPE // rank
+    extra = -(-rot_rows // 16) * 16
     packed = jnp.concatenate(
         [
             kv_lat,
-            jnp.zeros((rows, NOPE), jnp.bfloat16),
-            key_rot,
-            jnp.zeros((rows, 128 - NOPE - ROPE), jnp.bfloat16),
+            key_rot.reshape(rot_rows, rank),
+            jnp.zeros((extra - rot_rows, rank), jnp.bfloat16),
         ],
-        axis=1,
+        axis=0,
     )
     q_lat = scaled_norm(jnp.dot(normed, q_down, preferred_element_type=jnp.float32), q_gain).astype(
         jnp.bfloat16
     )
-    swap = [(place, sp_count - 1 - place) for place in range(sp_count)]
     latents, q_group = gather(packed, q_lat)
+    turned = latents[:, rows : rows + rot_rows].reshape(-1, ROPE)
+    turned = jnp.pad(turned, ((0, 0), (NOPE, HEAD_KV - NOPE - ROPE)))
     mate = sp_count - 1 - sp_place
     base = jnp.stack([sp_place * group_rows, mate * group_rows + half])
     position = (
@@ -507,19 +648,12 @@
         jnp.sin(angles),
         position.astype(jnp.int32)[None, :],
         latents,
+        turned,
         kv_up,
         v_up.reshape(heads * VDIM, rank),
         rows,
     )
-    own_heads = lax.all_to_all(
-        attended.reshape(2, tp_count, half, heads * VDIM),
-        "tp",
-        split_axis=1,
-        concat_axis=3,
-        tiled=True,
-    )
-    returned = lax.ppermute(own_heads[1, 0], "sp", swap)
-    own_rows = jnp.concatenate([own_heads[0, 0], returned], axis=0)
+    own_rows = deliver(attended)
     projected = jnp.dot(own_rows, out_weight, preferred_element_type=jnp.float32)
     return scaled_norm(projected, out_gain).astype(jnp.bfloat16)
 

time: 220 us -> 171 us (0.78)
  Pallas kernels: 172 us -> 134 us
  blocking collectives: 11.2 us -> 0 us
  waiting for transfers between devices: 9.62 us -> 0 us
  local copies, waits for them, and re-layouts: 3.23 us -> 12.1 us
  matrix products: 14.1 us -> 16.7 us
    pallas_call x1, Pallas kernels: 97.2 us -> 66.5 us  [gather(): pl.pallas_call(functools.partial(gather_kernel, sp_count, tp_count), out_...]
    pallas_call x1, Pallas kernels: 74.7 us -> 54.1 us  [attend(): pl.pallas_call(functools.partial(attend_kernel, rows, heads, group_rows,...]
    pallas_call x0 -> x1, Pallas kernels: none -> 13.6 us  [deliver(): pl.pallas_call(functools.partial(deliver_kernel, sp_count, tp_count), out...]
    all_to_all x1 -> x0, blocking collectives: 11.2 us -> none  [local(): lax.all_to_all(attended.reshape(2, tp_count, half, heads * VDIM), 'tp', s...]
    ppermute x1 -> x0, waiting for transfers between devices: 9.62 us -> none  [local(): returned = lax.ppermute(own_heads[1, 0], 'sp', swap)]
    unnamed x27 -> x23, local copies, waits for them, and re-layouts: 1.73 us -> 5.31 us
    pad x0 -> x1, local copies, waits for them, and re-layouts: none -> 2.31 us  [local(): turned = jnp.pad(turned, ((0, 0), (NOPE, HEAD_KV - NOPE - ROPE)))]
  transfers between devices with their start and end apart: 1 -> 0, of which waited for: 1 -> 0; matrix products, arithmetic and copies ran while one was open for 0% -> 0% of each run, Pallas kernels for 0% -> 0%
where the time goes in v3:
time: 171 us; the launch traced here: 170 us
  Pallas kernels  134 us (78%)
  matrix products  16.7 us (10%)
  local copies, waits for them, and re-layouts  12.1 us (7%)
  other arithmetic  7.32 us (4%)
    pallas_call x1, Pallas kernels, gather(): pl.pallas_call(functools.partial(gather_kernel, sp_count, tp_count), out_...  66.5 us
    pallas_call x1, Pallas kernels, attend(): pl.pallas_call(functools.partial(attend_kernel, rows, heads, group_rows,...  54.1 us
    pallas_call x1, Pallas kernels, deliver(): pl.pallas_call(functools.partial(deliver_kernel, sp_count, tp_count), out...  13.6 us
    dot_general x1, matrix products, local(): jnp.dot(own_rows, out_weight, preferred_element_type=jnp.float32)  6.01 us
    unnamed x23, local copies, waits for them, and re-layouts  5.31 us
    dot_general x1, matrix products, local(): jnp.dot(normed, q_down, preferred_element_type=jnp.float32)  4.73 us
    dot_general x1, matrix products, local(): jnp.dot(normed, kv_down, preferred_element_type=jnp.float32)  3.57 us

profile of v3, /device:TPU:0, one launch (start us, length us, event | category | flops | bytes accessed | tf_op | source)
XLA Modules:
  0.0 170.3 jit_solution(14205449335710824426)
XLA Ops:
  0.0 2.2 %fusion = f32[256]{0:T(256)S(1)} fusion(bf16[256,4096]{1,0:T(8,128)(2,1)} %param.11), kind=kLoop, calls=%fused_computation.2 | loop fusion | flops 3145472 | bytes 2098176 | tf_op jit(solution)/shard_map/reduce_sum | solution.py:27
  2.3 2.4 %fusion.14 = f32[256,32]{0,1:T(8,128)S(1)} fusion(bf16[4096,32]{0,1:T(8,128)(2,1)S(1)} %copy-done, bf16[256,4096]{1,0:T(8,128)(2,1)} %param.11, f32[4096]{0:T(1024)} %param.12, f32[256]{0:T(256)S(1)} %add_rsqrt_fusion.3), kind=kOutput, calls=%fused_computation.38 | convolution fusion | flops 71303168 | bytes 2409472 | tf_op jit(solution)/shard_map/dot_general | solution.py:614
  4.7 0.1 fusion.8
  4.9 0.1 convert_element_type.43
  5.1 3.6 %multiply_reduce_fusion.2 = (f32[256]{0:T(256)S(1)}, f32[256,512]{1,0:T(8,128)S(1)}) fusion(bf16[4096,512]{1,0:T(8,128)(2,1)} %param.14, bf16[256,4096]{1,0:T(8,128)(2,1)S(1)} %copy-done.6, f32[4096]{0:T(1024)S(1)} %copy-done.10, f32[256]{0:T(256)S(1)} %add_rsqrt_fusion.3), kind=kOutput, calls=%fused_computation.10 | convolution fusion | flops 1078198016 | bytes 6834176 | tf_op jit(solution)/shard_map/dot_general | solution.py:611
  8.8 0.7 pad_maximum_fusion.lat_ref
  9.6 4.7 %multiply_reduce_fusion.1 = (f32[256]{0:T(256)S(1)}, f32[256,768]{1,0:T(8,128)S(1)}) fusion(bf16[4096,768]{1,0:T(8,128)(2,1)} %param.13, bf16[256,4096]{1,0:T(8,128)(2,1)S(1)} %copy-done.6, f32[4096]{0:T(1024)S(1)} %copy-done.10, f32[256]{0:T(256)S(1)} %add_rsqrt_fusion.3), kind=kOutput, calls=%fused_computation.8 | convolution fusion | flops 1615200000 | bytes 9193472 | tf_op jit(solution)/shard_map/dot_general | solution.py:626
  14.3 0.9 multiply_convert_fusion.1.q_ref
  15.2 66.5 %shard_map.109 = (bf16[32,272,512]{2,1,0:T(8,128)(2,1)}, bf16[2,4,128,768]{3,2,1,0:T(8,128)(2,1)}) custom-call(bf16[272,512]{1,0:T(8,128)(2,1)} %pad_maximum_fusion.lat_ref, bf16[256,768]{1,0:T(8,128)(2,1)} %multiply_convert_fusion.1.q_ref), custom_call_target="tpu_custom_call" | custom-call | bytes 35651584 | tf_op jit(solution)/shard_map/pallas_call | solution.py:489
  81.7 1.1 slice.14
  82.7 2.2 %reshape.141 = bf16[8192,32]{1,0:T(8,128)(2,1)} reshape(bf16[32,16,512]{2,1,0:T(8,128)(2,1)S(1)} %slice.14) | data formatting | bytes 1048576 | tf_op jit(solution)/shard_map/reshape | solution.py:630
  84.9 2.3 %pad.4.turned_ref = bf16[8192,128]{1,0:T(8,128)(2,1)S(1)} pad(bf16[8192,32]{1,0:T(8,128)(2,1)} %reshape.141, bf16[]{:T(256)} %constant.44.clone.1), padding=0_0x64_32 | pad | bytes 2621442 | tf_op jit(solution)/shard_map/jit(_pad)/pad | solution.py:631
  87.5 0.9 multiply_sine_fusion
  88.5 0.2 copy.18
  88.7 0.7 slice.18
  89.4 1.3 copy.16
  90.7 0.9 copy-done.3
  91.7 0.8 copy-done.4
  92.5 1.4 copy-done.5
  93.9 54.1 %shard_map.110.in_ref = bf16[1024,256]{1,0:T(8,128)(2,1)S(1)} custom-call(s32[2]{0:T(128)S(1)} %pad_add_fusion.place_ref, bf16[1024,768]{1,0:T(8,128)(2,1)S(1)} %bitcast.22, bf16[4,96,768]{2,1,0:T(8,128)(2,1)S(1)} %bitcast.19, f32[16,1024]{1,0:T(8,128)S(1)} %copy-done.4, f32[16,1024]{1,0:T(8,128)S(1)} %get-tuple-element.11.sin_ref, s32[1,1024]{1,0:T(1,128)S(1)} %bitcast.21, ...), custom_call_target="tpu_custom_call" | custom-call | flops 10737418240 | bytes 8912896 | tf_op jit(solution)/shard_map/pallas_call | solution.py:200
  148.0 0.8 copy-done.2
  148.8 13.6 %shard_map.111 = bf16[256,1024]{1,0:T(8,128)(2,1)} custom-call(bf16[1024,256]{1,0:T(8,128)(2,1)} %copy-done.2), custom_call_target="tpu_custom_call" | custom-call | tf_op jit(solution)/shard_map/pallas_call | solution.py:568
  162.4 6.0 %multiply_reduce_fusion = (f32[256]{0:T(256)S(1)}, f32[256,4096]{1,0:T(8,128)S(1)}) fusion(bf16[256,1024]{1,0:T(8,128)(2,1)} %shard_map.111, bf16[1024,4096]{1,0:T(8,128)(2,1)} %param.20), kind=kOutput, calls=%fused_computation.6 | convolution fusion | flops 2149580544 | bytes 13108224 | tf_op jit(solution)/shard_map/dot_general | solution.py:657
  168.4 1.9 %multiply_convert_fusion = bf16[256,4096]{1,0:T(8,128)(2,1)} fusion(f32[256,4096]{1,0:T(8,128)S(1)} %get-tuple-element.20, f32[4096]{0:T(1024)S(1)} %copy-done.7, f32[256]{0:T(256)S(1)} %add_rsqrt_fusion), kind=kLoop, calls=%fused_computation.5 | loop fusion | flops 3145728 | bytes 6308864 | tf_op jit(solution)/shard_map/convert_element_type | solution.py:658
  (32 shorter events, 0.6 us)
Async XLA Ops:
  0.0 2.3 %copy-start = (bf16[4096,32]{0,1:T(8,128)(2,1)S(1)}, bf16[4096,32]{0,1:T(8,128)(2,1)}, u32[]{:S(2)}) copy-start(bf16[4096,32]{0,1:T(8,128)(2,1)} %param.15) | copy-start | bytes 786436
  0.0 5.1 %copy-start.6 = (bf16[256,4096]{1,0:T(8,128)(2,1)S(1)}, bf16[256,4096]{1,0:T(8,128)(2,1)}, u32[]{:S(2)}) copy-start(bf16[256,4096]{1,0:T(8,128)(2,1)} %param.11) | copy-start | bytes 6291460
  0.0 5.1 %copy-start.10 = (f32[4096]{0:T(1024)S(1)}, f32[4096]{0:T(1024)}, u32[]{:S(2)}) copy-start(f32[4096]{0:T(1024)} %param.12) | copy-start | bytes 49156
  5.1 3.6 %copy-start.9 = (f32[512]{0:T(512)S(1)}, f32[512]{0:T(512)}, u32[]{:S(2)}) copy-start(f32[512]{0:T(512)} %param.17) | copy-start | bytes 6148
  9.6 4.7 %copy-start.8 = (f32[768]{0:T(1024)S(1)}, f32[768]{0:T(1024)}, u32[]{:S(2)}) copy-start(f32[768]{0:T(1024)} %param.16) | copy-start | bytes 9220
  15.2 73.3 %copy-start.1 = (bf16[512,512]{1,0:T(8,128)(2,1)S(1)}, bf16[512,512]{1,0:T(8,128)(2,1)}, u32[]{:S(2)}) copy-start(bf16[512,512]{1,0:T(8,128)(2,1)} %kv_up_ref.1) | copy-start | bytes 1572868
  90.7 1.0 copy-start.3
  91.7 0.8 copy-start.4
  92.5 1.4 copy-start.5
  148.0 0.8 copy-start.2
  162.4 6.0 %copy-start.7 = (f32[4096]{0:T(1024)S(1)}, f32[4096]{0:T(1024)}, u32[]{:S(2)}) copy-start(f32[4096]{0:T(1024)} %param.21) | copy-start | bytes 49156
